TPU v7x, 32 devices: a whole 2x2x4 slice. The times are simulated.
32 devices in a mesh: ep: 16 (over z, y, x), tp: 2 (over core).
Axes of the slice: x: 2, y: 2, z: 4, core: 2. Of those that a mesh axis runs over, the one named last changes fastest.
Arguments:
- tokens: bfloat16 [384, 2048], P('ep'), may hold values from -6 to 6
- norm_gain: bfloat16 [2048], replicated, may hold values from 0.099609375 to 1.8984375
- query_w: bfloat16 [2048, 1024], P(None, 'tp'), may hold values from -0.125 to 0.125
- key_w: bfloat16 [2048, 128], replicated, may hold values from -0.125 to 0.125
- value_w: bfloat16 [2048, 128], replicated, may hold values from -0.125 to 0.125
- forget_w: bfloat16 [2048, 16], replicated, may hold values from -0.125 to 0.125
- forget_bias: float32 [16], replicated, may hold values from 0 to 4
- query_gain: bfloat16 [64], replicated, may hold values from 0.099609375 to 1.8984375
- key_gain: bfloat16 [64], replicated, may hold values from 0.099609375 to 1.8984375
- cache_key: bfloat16 [384, 2, 64, 1024], P('ep', 'tp'), may hold values from -6 to 6
- cache_value: bfloat16 [384, 2, 64, 1024], P('ep', 'tp'), may hold values from -6 to 6
- cache_gate: float32 [384, 16, 1024], P('ep', 'tp'), may hold values from -105 to 0, as said below
- cache_len: int32 [384], P('ep'), may hold values from 256 to 1024
- out_w: bfloat16 [1024, 2048], P('tp'), may hold values from -0.1875 to 0.1875
- post_gain: bfloat16 [2048], replicated, may hold values from 0.099609375 to 1.8984375
- branch_gate: bfloat16 [2048], replicated, may hold values from -0.125 to 0.125
- dense_gate_w: bfloat16 [2048, 16384], P(None, ('ep', 'tp')), may hold values from -0.125 to 0.125
- dense_up_w: bfloat16 [2048, 16384], P(None, ('ep', 'tp')), may hold values from -1.3258252 to 1.3258252
- dense_down_w: bfloat16 [16384, 2048], P(('ep', 'tp')), may hold values from -0.046875 to 0.046875
- expert_choice: int32 [384, 2], P('ep'), may hold values from 0 to 15, as said below
- route_weight: float32 [384, 2], P('ep'), may hold values from 0.1 to 1
- expert_gate_w: bfloat16 [16, 2048, 1024], P('ep', None, 'tp'), may hold values from -0.125 to 0.125
- expert_up_w: bfloat16 [16, 2048, 1024], P('ep', None, 'tp'), may hold values from -0.125 to 0.125
- expert_down_w: bfloat16 [16, 1024, 2048], P('ep', 'tp'), may hold values from -0.1875 to 0.1875
Outputs:
- mixed_out: bfloat16 [384, 2048], P('ep', 'tp')
- fresh_key: bfloat16 [384, 2, 64], P('ep', 'tp')
- fresh_value: bfloat16 [384, 2, 64], P('ep', 'tp')
- fresh_gate: float32 [384, 16], P('ep', 'tp')
Inputs may be any that keep to these rules, and one draw needn't show every extreme that they name: `cache_gate`: Non-increasing along positions. `expert_choice`: experts 4 * g to 4 * g + 3 form group g. A token names 2 different experts of one group. Among the 24 tokens of one index of ep, those at even offsets all choose one group and the others choose other groups; no expert is named more than 6 times by them, and some expert exactly 6 times.
All inputs are finite; a program needn't handle non-finite values.
Results may differ from a plain program's by a relative error of at most 0.014.
Values may be sent and summed in bfloat16 or wider, within the bound.
No kernel may reach another device: no remote copies, remote signals or barrier semaphores. Data moves between devices by JAX's collectives and lax.ppermute only.
A program may use at most 128 MiB of HBM per device.

v0:
```python
import functools

import jax
import jax.numpy as jnp
from jax import lax
from jax.experimental import pallas as pl
from jax.experimental.pallas import tpu as pltpu
from jax.sharding import PartitionSpec as P


GROUPS = 4
LANES = 128
BLOCK_KEY = 1024.0

norm_eps = 1e-06


def rms_scale(values, gain_vec):
    mean_square = jnp.mean(values * values, axis=-1, keepdims=True)
    return values * lax.rsqrt(mean_square + norm_eps) * gain_vec


def split_two(values):
    high = values.astype(jnp.bfloat16)
    low = (values - high.astype(jnp.float32)).astype(jnp.bfloat16)
    return high, low


def route_slots(expert_choice, ep_count, capacity):
    route_ids = expert_choice.reshape(-1)
    member = (route_ids[:, None] == jnp.arange(ep_count)[None, :]).astype(jnp.float32)
    count = route_ids.shape[0]
    earlier = (
        lax.broadcasted_iota(jnp.int32, (count, count), 0)
        > lax.broadcasted_iota(jnp.int32, (count, count), 1)
    ).astype(jnp.float32)
    before = jnp.dot(earlier, member, preferred_element_type=jnp.float32)
    rank = jnp.sum(before * member, axis=1)
    slot = route_ids.astype(jnp.float32) * capacity + rank
    return slot.reshape(expert_choice.shape)


F32, BF16 = jnp.float32, jnp.bfloat16
VMEM = pl.BlockSpec(memory_space=pltpu.VMEM)
SMEM = pl.BlockSpec(memory_space=pltpu.SMEM)


def call(kernel, outs, operands, hbm=(), scratch=(), limit=20):
    specs = []
    held = []
    for index, op in enumerate(operands):
        if index in hbm:
            specs.append(pl.BlockSpec(memory_space=pltpu.HBM))
            held.append(pltpu.with_memory_space_constraint(op, pltpu.HBM))
        elif op.dtype == jnp.int32 and op.ndim == 1:
            specs.append(SMEM)
            held.append(op)
        else:
            specs.append(VMEM)
            held.append(pltpu.with_memory_space_constraint(op, pltpu.VMEM))
    return pl.pallas_call(
        kernel,
        in_specs=specs,
        out_specs=[VMEM] * len(outs),
        out_shape=[pltpu.VMEM(shape, dtype) for shape, dtype in outs],
        scratch_shapes=list(scratch),
        compiler_params=pltpu.CompilerParams(vmem_limit_bytes=limit * 1024 * 1024),
    )(*held)


def axis_iota(shape, axis):
    return lax.broadcasted_iota(jnp.int32, shape, axis).astype(F32)


def block_of(index, size):
    return jnp.floor((index + 0.5) * (1.0 / size))


def dot(left, right):
    return jnp.dot(left, right, preferred_element_type=F32)


def high_low(values):
    high = values.astype(BF16).astype(F32)
    return high, values - high


def to_row(column):
    rows = column.shape[0]
    wide = jnp.broadcast_to(column, (rows, LANES))
    if rows < LANES:
        wide = jnp.concatenate([wide, jnp.zeros((LANES - rows, LANES), F32)], axis=0)
    return jnp.transpose(wide)[0:1]


def silu(values):
    return values / (1.0 + jnp.exp(-values))


def post_kernel(ids, tokens, part_a, part_b, gain, branch_gate, notes, payload, resid, branch):
    half = resid.shape[1]
    first = ids[0] == 0
    total = tokens[...].astype(F32) + (part_a[...].astype(F32) + part_b[...].astype(F32))
    total = total.astype(BF16).astype(F32)
    mean_square = jnp.mean(total * total, axis=-1, keepdims=True)
    post = (total * lax.rsqrt(mean_square + norm_eps) * gain[...].astype(F32)[None]).astype(BF16)
    gate = jnp.sum(post.astype(F32) * branch_gate[...].astype(F32)[None], axis=-1, keepdims=True)
    branch[...] = jnp.broadcast_to(1.0 / (1.0 + jnp.exp(-gate)), branch.shape)
    payload[:, :half] = jnp.where(first, post[:, :half], post[:, half:])
    payload[:, half:] = notes[...]
    resid[...] = jnp.where(first, total[:, :half], total[:, half:]).astype(BF16)


def load_kernel(
    ids, column, gate_in, up_in, expert_gate_in, expert_up_in, down_in, expert_in,
    combine, gate_w, up_w, expert_gate, expert_up, down_own, expert_own, down_sent, sems,
    *, seq, capacity, top_k,
):
    hidden, half = down_own.shape
    other = expert_own.shape[0]
    mine = pl.ds(pl.multiple_of(ids[0] * half, half), half)
    theirs = pl.ds(pl.multiple_of((1 - ids[0]) * half, half), half)
    pairs = [
        (down_in.at[:, theirs], down_sent.at[pl.ds(0, hidden)]),
        (expert_in.at[:, theirs], down_sent.at[pl.ds(hidden, other)]),
        (gate_in, gate_w), (up_in, up_w), (expert_gate_in, expert_gate),
        (expert_up_in, expert_up), (down_in.at[:, mine], down_own),
        (expert_in.at[:, mine], expert_own),
    ]
    copies = [pltpu.make_async_copy(a, b, sems.at[i]) for i, (a, b) in enumerate(pairs)]
    for copy in copies:
        copy.start()
    plane = combine.shape[0]
    planes = combine.shape[2] // capacity
    pair_rows = combine.shape[1] // planes
    tokens = planes * seq
    info = column[:, column.shape[1] - LANES :].astype(F32)
    near_key = block_of(axis_iota((tokens, 1), 0), seq) * BLOCK_KEY
    lane = axis_iota((1, planes * capacity), 1)
    lane_block = block_of(lane, capacity)
    lane_key = lane_block * BLOCK_KEY + (lane - lane_block * capacity)
    pair = axis_iota((planes * pair_rows, 1), 0)
    pair_block = block_of(pair, pair_rows)
    pair_offset = pair - pair_block * pair_rows
    pair_id = jnp.where(pair_offset < seq // 2, pair_block * (seq // 2) + pair_offset, -1.0)
    joined = (block_of(axis_iota((1, tokens), 1), 2) == pair_id).astype(BF16)
    for j in range(plane):
        match = jnp.zeros((tokens, planes * capacity), F32)
        for k in range(top_k):
            match = match + (
                info[:, k : k + 1] + near_key == lane_key + ids[2 + j].astype(F32)
            ).astype(F32)
        combine[j] = dot(joined, match.astype(BF16)).astype(BF16)
    for copy in copies:
        copy.wait()


def hidden_kernel(ids, *refs, seq, capacity, top_k):
    plane = (len(refs) - 9) // 2
    owns, others = refs[:plane], refs[plane : 2 * plane]
    gate_w, up_w, expert_gate, expert_up, out, slot_weight, lefts, rights, notes = refs[2 * plane :]
    count, half = lefts.shape
    slots = slot_weight.shape[0]
    group = count // plane
    for j in range(plane):
        rows = pl.ds(j * group, group)
        lefts[rows, :] = owns[j][:, :half]
        rights[rows, :] = others[j][:, :half]
        notes[rows, :] = owns[j][:, half:].astype(F32)
    own_rows = pl.ds(pl.multiple_of(ids[0] * half, half), half)
    other_rows = pl.ds(pl.multiple_of((1 - ids[0]) * half, half), half)
    left = lefts[...]
    right = rights[...]

    def project(rows_own, rows_other, weight):
        return dot(rows_own, weight[own_rows, :]) + dot(rows_other, weight[other_rows, :])

    hidden = silu(project(left, right, gate_w)) * project(left, right, up_w)
    out[0:count, 0 : gate_w.shape[1]] = hidden.astype(BF16)
    squares = jnp.sum(hidden * hidden, axis=1, keepdims=True)
    tile_row = lax.broadcasted_iota(jnp.int32, (2 * plane, LANES), 0)
    tile = jnp.zeros((2 * plane, LANES), F32)
    for j in range(plane):
        high, low = high_low(to_row(squares[j * group : (j + 1) * group]))
        tile = jnp.where(tile_row == 2 * j, high, jnp.where(tile_row == 2 * j + 1, low, tile))
    out[count + slots :, :] = jnp.zeros((2 * plane, out.shape[1]), BF16)
    out[count + slots :, 0:LANES] = tile.astype(BF16)

    turned = jnp.transpose(notes[...])
    token = axis_iota((1, count), 1)
    token_key = block_of(token, seq) * BLOCK_KEY
    slot = axis_iota((slots, 1), 0)
    slot_block = block_of(slot, capacity)
    slot_key = slot_block * BLOCK_KEY + (slot - slot_block * capacity) + ids[1].astype(F32)
    pick = jnp.zeros((slots, count), F32)
    weight = jnp.zeros((slots, count), F32)
    for k in range(top_k):
        hit = (turned[k : k + 1] + token_key == slot_key).astype(F32)
        value = turned[top_k + k : top_k + k + 1] + turned[2 * top_k + k : 2 * top_k + k + 1]
        pick = pick + hit
        weight = weight + hit * value
    slot_weight[...] = jnp.broadcast_to(
        jnp.sum(weight, axis=1, keepdims=True), slot_weight.shape
    )
    pick = pick.astype(BF16)
    rows_own = dot(pick, left).astype(BF16)
    rows_other = dot(pick, right).astype(BF16)
    active = silu(project(rows_own, rows_other, expert_gate)) * project(
        rows_own, rows_other, expert_up
    )
    out[count : count + slots, 0 : expert_gate.shape[1]] = active.astype(BF16)


def down_kernel(own, other, down_own, expert_own, down_got, slot_weight, *outs, count):
    plane = len(outs)
    half = outs[0].shape[1]
    slots = slot_weight.shape[0]
    hidden, routed_hidden = down_own.shape[0], expert_own.shape[0]
    dense = dot(own[0:count, 0:hidden], down_own[...]) + dot(
        other[0:count, 0:hidden], down_got[0:hidden, :]
    )
    routed_rows = slice(count, count + slots)
    routed = dot(own[routed_rows, 0:routed_hidden], expert_own[...]) + dot(
        other[routed_rows, 0:routed_hidden], down_got[hidden:, :]
    )
    routed = routed * slot_weight[:, 0:1]
    squares = own[count + slots :, 0:LANES].astype(F32) + other[count + slots :, 0:LANES].astype(F32)
    group, part = count // plane, slots // plane
    tile_row = lax.broadcasted_iota(jnp.int32, (8, LANES), 0)
    for j in range(plane):
        outs[j][0:group, :] = dense[j * group : (j + 1) * group].astype(BF16)
        outs[j][group : group + part, :] = routed[j * part : (j + 1) * part].astype(BF16)
        high, low = high_low(squares[2 * j : 2 * j + 1] + squares[2 * j + 1 : 2 * j + 2])
        outs[j][group + part :, :] = jnp.zeros((8, half), BF16)
        outs[j][group + part :, 0:LANES] = jnp.where(
            tile_row == 0, high, jnp.where(tile_row == 1, low, 0.0)
        ).astype(BF16)


def plane_kernel(*refs, planes, seq, capacity):
    plane = len(refs) - planes - 1
    parts, combine, outs = refs[:plane], refs[plane], refs[plane + 1 :]
    group, part = planes * seq, planes * capacity
    dense = parts[0][0:group, :].astype(F32)
    routed = dot(combine[0], parts[0][group : group + part, :])
    notes = parts[0][group + part :, 0:LANES].astype(F32)
    for j in range(1, plane):
        dense = dense + parts[j][0:group, :].astype(F32)
        routed = routed + dot(combine[j], parts[j][group : group + part, :])
        notes = notes + parts[j][group + part :, 0:LANES].astype(F32)
    high, low = high_low(notes[0:1] + notes[1:2])
    pair_rows = combine.shape[1] // planes
    tile_row = lax.broadcasted_iota(jnp.int32, (pair_rows, LANES), 0)
    for k in range(planes):
        outs[k][0:seq, :] = dense[k * seq : (k + 1) * seq].astype(BF16)
        tail = routed[k * pair_rows : (k + 1) * pair_rows]
        first = jnp.where(
            tile_row == seq // 2,
            high,
            jnp.where(tile_row == seq // 2 + 1, low, tail[:, 0:LANES]),
        )
        outs[k][seq:, 0:LANES] = first.astype(BF16)
        outs[k][seq:, LANES:] = tail[:, LANES:].astype(BF16)


def final_kernel(*refs, ff_total, route_base, top_k):
    planes = len(refs) - 5
    ids, parts = refs[0], refs[1 : 1 + planes]
    resid, branch, notes, out = refs[1 + planes :]
    seq = resid.shape[0]
    half_seq = seq // 2
    pair_rows = parts[0].shape[0] - seq
    group = block_of(notes[:, 0:1].astype(F32), route_base)
    token_pair = block_of(axis_iota((seq, 1), 0), 2)
    lane = axis_iota((1, pair_rows), 1)
    dense = jnp.zeros(out.shape, F32)
    routed = jnp.zeros(out.shape, F32)
    squares = jnp.zeros((seq, LANES), F32)
    for k in range(planes):
        dense = dense + parts[k][0:seq, :].astype(F32)
        tail = parts[k][seq:, :]
        place = jnp.where(
            (token_pair == lane) & (group == ids[k].astype(F32)), 1.0, 0.0
        ).astype(BF16)
        routed = routed + dot(place, tail)
        values = tail[:, 0:LANES].astype(F32)
        row = values[half_seq : half_seq + 1] + values[half_seq + 1 : half_seq + 2]
        turned = jnp.transpose(jnp.broadcast_to(row, (LANES, LANES)))
        squares = squares + turned[k * seq : (k + 1) * seq]
    scale = branch[:, 0:1] * lax.rsqrt(squares[:, 0:1] * (1.0 / ff_total) + norm_eps)
    out[...] = (resid[...].astype(F32) + routed + scale * dense).astype(BF16)


def attend_kernel(
    ids, lens, tokens_in, norm_in, query_in, key_in, bias_in,
    query_w, key_w, value_w, forget_w, cache_key, cache_value, cache_gate, out_w,
    partial, fresh_key, fresh_value, fresh_gate,
    q_w, k_w, v_w, f_w, keys, values, gates, o_w, q_rows, k_rows, v_rows, f_cols, g_cols, mixed,
    tokens, norm_gain, query_gain, key_gain, forget_bias, sems,
    *, heads, chunks,
):
    seq = tokens.shape[0]
    head = cache_key.shape[1]
    span = cache_key.shape[2]
    step = seq // chunks
    plain = [
        (tokens_in, tokens), (norm_in, norm_gain), (query_in, query_gain), (key_in, key_gain),
        (bias_in, forget_bias), (key_w, k_w), (value_w, v_w), (forget_w, f_w), (query_w, q_w),
    ]
    small = [pltpu.make_async_copy(a, b, sems.at[i]) for i, (a, b) in enumerate(plain)]
    base = len(small)
    parts = []
    for c in range(chunks):
        rows = pl.ds(c * step, step)
        for a, b in ((cache_key, keys), (cache_gate, gates), (cache_value, values)):
            parts.append(pltpu.make_async_copy(a.at[rows], b.at[rows], sems.at[base + len(parts)]))
    last = pltpu.make_async_copy(out_w, o_w, sems.at[base + len(parts)])
    for copy in small + parts + [last]:
        copy.start()
    for copy in small[:5]:
        copy.wait()
    small = small[5:]
    first = ids[0] == 0
    resid = tokens[...].astype(F32)
    mean_square = jnp.mean(resid * resid, axis=-1, keepdims=True)
    normed = (resid * lax.rsqrt(mean_square + norm_eps) * norm_gain[...].astype(F32)[None]).astype(BF16)
    small[0].wait()
    key = dot(normed, k_w[...])
    key = jnp.where(first, key[:, :head], key[:, head:])
    key = rms_scale(key, key_gain[...].astype(F32)[None]).astype(BF16)
    fresh_key[...] = key
    k_rows[...] = key.astype(F32)
    small[1].wait()
    value = dot(normed, v_w[...])
    value = jnp.where(first, value[:, :head], value[:, head:]).astype(BF16)
    fresh_value[...] = value
    v_rows[...] = value.astype(F32)
    small[2].wait()
    forget = lax.dot_general(
        normed, f_w[...], (((1,), (1,)), ((), ())), preferred_element_type=F32
    )
    forget = forget + forget_bias[...][None]
    forget = jnp.minimum(forget, 0.0) - jnp.log1p(jnp.exp(-jnp.abs(forget)))
    forget = jnp.where(first, forget[:, :heads], forget[:, heads:])
    wide = jnp.concatenate([forget, jnp.zeros((seq, LANES - heads), F32)], axis=1)
    wide = jnp.concatenate([wide, jnp.zeros((LANES - seq, LANES), F32)], axis=0)
    f_cols[...] = jnp.transpose(wide)[0:heads]
    small[3].wait()
    queries = dot(normed, q_w[...])
    for h in range(heads):
        part = queries[:, h * head : (h + 1) * head]
        part = rms_scale(part, query_gain[...].astype(F32)[None]).astype(BF16)
        q_rows[:, h, :] = part.astype(F32)
    g_cols[...] = jnp.zeros(g_cols.shape, F32)
    lane = lax.broadcasted_iota(jnp.int32, (heads, span), 1)
    lane_small = lax.broadcasted_iota(jnp.int32, (heads, LANES), 1)
    scale = head ** (-0.5)

    def one(s):
        length = lens[s]
        place = length - 1
        block = pl.multiple_of((place // LANES) * LANES, LANES)
        near = gates[s, :, pl.ds(block, LANES)]
        previous = jnp.sum(
            jnp.where(lane_small == place - block, near, 0.0), axis=1, keepdims=True
        )
        log_forget = f_cols[:, s : s + 1]
        current = previous + log_forget
        g_cols[:, s : s + 1] = current
        query = q_rows[s]
        own = jnp.sum(query * k_rows[s : s + 1], axis=1, keepdims=True) * scale
        logits = dot(query.astype(BF16), keys[s]) * scale + (current - gates[s])
        logits = jnp.where(lane < length, logits, -1e30)
        top = jnp.maximum(jnp.max(logits, axis=1, keepdims=True), own)
        weight = jnp.exp(logits - top)
        own_weight = jnp.exp(own - top)
        total = jnp.sum(weight, axis=1, keepdims=True) + own_weight
        inverse = 1.0 / total
        probs = (weight * inverse).astype(BF16)
        own_prob = (own_weight * inverse).astype(BF16).astype(F32)
        out = lax.dot_general(
            probs, values[s], (((1,), (1,)), ((), ())), preferred_element_type=F32
        )
        mixed[s] = out + own_prob * v_rows[s : s + 1]

    for c in range(chunks):
        for copy in parts[3 * c : 3 * c + 3]:
            copy.wait()
        for s in range(c * step, (c + 1) * step):
            one(s)
    turned = jnp.concatenate([g_cols[...], jnp.zeros((LANES - heads, LANES), F32)], axis=0)
    fresh_gate[...] = jnp.transpose(turned)[0:seq, 0:heads]
    last.wait()
    total = jnp.zeros(partial.shape, F32)
    for h in range(heads):
        total = total + dot(mixed[:, h, :].astype(BF16), o_w[h * head : (h + 1) * head, :])
    partial[...] = total.astype(BF16)


def attend(
    ids, tokens, norm_gain, query_w, key_w, value_w, forget_w, forget_bias,
    query_gain, key_gain, cache_key, cache_value, cache_gate, cache_len, out_w,
):
    seq, width = tokens.shape
    heads = cache_gate.shape[1]
    head, span = cache_key.shape[2:]
    chunks = 3 if seq % 3 == 0 else 1
    scratch = [
        pltpu.VMEM(query_w.shape, BF16), pltpu.VMEM(key_w.shape, BF16),
        pltpu.VMEM(value_w.shape, BF16), pltpu.VMEM(forget_w.shape[::-1], BF16),
        pltpu.VMEM((seq, head, span), BF16), pltpu.VMEM((seq, head, span), BF16),
        pltpu.VMEM((seq, heads, span), F32), pltpu.VMEM(out_w.shape, BF16),
        pltpu.VMEM((seq, heads, head), F32), pltpu.VMEM((seq, head), F32),
        pltpu.VMEM((seq, head), F32), pltpu.VMEM((heads, LANES), F32),
        pltpu.VMEM((heads, LANES), F32), pltpu.VMEM((seq, heads, head), F32),
        pltpu.VMEM(tokens.shape, BF16), pltpu.VMEM(norm_gain.shape, BF16),
        pltpu.VMEM(query_gain.shape, BF16), pltpu.VMEM(key_gain.shape, BF16),
        pltpu.VMEM(forget_bias.shape, F32),
        pltpu.SemaphoreType.DMA((10 + 3 * chunks,)),
    ]
    partial, fresh_key, fresh_value, current = call(
        functools.partial(attend_kernel, heads=heads, chunks=chunks),
        [((seq, width), BF16), ((seq, head), BF16), ((seq, head), BF16), ((seq, heads), F32)],
        [
            ids, cache_len, tokens, norm_gain, query_gain, key_gain, forget_bias, query_w, key_w, value_w, forget_w.T,
            cache_key[:, 0], cache_value[:, 0], cache_gate, out_w,
        ],
        hbm=range(2, 15),
        scratch=scratch,
        limit=32,
    )
    return partial, fresh_key[:, None], fresh_value[:, None], current


def body(
    tokens, norm_gain, query_w, key_w, value_w, forget_w, forget_bias, query_gain, key_gain,
    cache_key, cache_value, cache_gate, cache_len, out_w, post_gain, branch_gate,
    dense_gate_w, dense_up_w, dense_down_w, expert_choice, route_weight,
    expert_gate_w, expert_up_w, expert_down_w,
):
    seq, width = tokens.shape
    tp_count = lax.axis_size("tp")
    ep_count = lax.axis_size("ep")
    tp_rank = lax.axis_index("tp")
    ep_rank = lax.axis_index("ep")
    half = width // tp_count
    planes = GROUPS
    plane = ep_count // planes
    capacity = 2 * ((seq + 2 * plane - 1) // (2 * plane))
    top_k = expert_choice.shape[1]
    ff_local = dense_gate_w.shape[1]
    expert_local = expert_gate_w.shape[2]
    widest = max(ff_local, expert_local)
    ff_total = ff_local * ep_count * tp_count
    count, slots = ep_count * seq, ep_count * capacity
    pair_rows = 8 * ((seq // 2 + 2 + 7) // 8)
    z_rank = ep_rank // plane
    p_rank = ep_rank % plane

    def swap(values):
        return lax.ppermute(values, "tp", [(i, 1 - i) for i in range(tp_count)])

    def exchange(values, mask):
        return lax.ppermute(values, "ep", [(i, i ^ mask) for i in range(ep_count)])

    slot_ids = route_slots(expert_choice, ep_count, capacity)
    weight_high, weight_low = split_two(route_weight)
    notes = jnp.concatenate([slot_ids.astype(BF16), weight_high, weight_low], axis=1)
    notes = jnp.pad(notes, ((0, 0), (0, LANES - notes.shape[1])))
    peers = jnp.bitwise_xor(jnp.arange(plane, dtype=jnp.int32), p_rank) + z_rank * plane
    ids = jnp.concatenate([jnp.stack([tp_rank, ep_rank * capacity]), peers * capacity])
    ids = ids.astype(jnp.int32)
    z_peers = jnp.bitwise_xor(jnp.arange(planes, dtype=jnp.int32), z_rank)

    partial, fresh_key, fresh_value, current = attend(
        ids, tokens, norm_gain, query_w, key_w, value_w, forget_w, forget_bias,
        query_gain, key_gain, cache_key, cache_value, cache_gate, cache_len, out_w,
    )
    payload, resid, branch = call(
        post_kernel,
        [((seq, half + LANES), BF16), ((seq, half), BF16), ((seq, LANES), F32)],
        [ids, tokens, partial, swap(partial), post_gain, branch_gate, notes],
    )
    column = jnp.concatenate(
        [payload] + [exchange(payload, k * plane) for k in range(1, planes)], axis=0
    )
    owns = [column] + [None] * (plane - 1)
    for j in reversed(range(1, plane)):
        owns[j] = exchange(column, j)
    combine, gate_w, up_w, expert_gate, expert_up, down_own, expert_own, down_sent = call(
        functools.partial(load_kernel, seq=seq, capacity=capacity, top_k=top_k),
        [((plane, planes * pair_rows, planes * capacity), BF16)]
        + [(dense_gate_w.shape, BF16)] * 2
        + [(expert_gate_w.shape[1:], BF16)] * 2
        + [((ff_local, half), BF16), ((expert_local, half), BF16)]
        + [((ff_local + expert_local, half), BF16)],
        [
            ids, column, dense_gate_w, dense_up_w, expert_gate_w[0], expert_up_w[0],
            dense_down_w, expert_down_w[0],
        ],
        hbm=range(2, 8),
        scratch=[pltpu.SemaphoreType.DMA((8,))],
    )
    down_got = swap(down_sent)
    others = [swap(values) for values in owns]
    hidden, slot_weight = call(
        functools.partial(hidden_kernel, seq=seq, capacity=capacity, top_k=top_k),
        [((count + slots + 2 * plane, widest), BF16), ((slots, LANES), F32)],
        [ids, *owns, *others, gate_w, up_w, expert_gate, expert_up],
        scratch=[
            pltpu.VMEM((count, half), BF16), pltpu.VMEM((count, half), BF16),
            pltpu.VMEM((count, LANES), F32),
        ],
    )
    sums = call(
        functools.partial(down_kernel, count=count),
        [((planes * (seq + capacity) + 8, half), BF16)] * plane,
        [
            hidden, swap(hidden), down_own, expert_own, down_got, slot_weight,
        ],
    )
    arrived = [sums[0]] + [None] * (plane - 1)
    for j in reversed(range(1, plane)):
        arrived[j] = exchange(sums[j], j)
    lasts = call(
        functools.partial(plane_kernel, planes=planes, seq=seq, capacity=capacity),
        [((seq + pair_rows, half), BF16)] * planes,
        [*arrived, combine],
    )
    final = [lasts[0]] + [exchange(lasts[k], k * plane) for k in range(1, planes)]
    (mixed_out,) = call(
        functools.partial(
            final_kernel, ff_total=ff_total, route_base=capacity * plane, top_k=top_k
        ),
        [((seq, half), BF16)],
        [z_peers, *final, resid, branch, notes],
    )
    return (mixed_out, fresh_key, fresh_value, current)


def solution(mesh):
    placed = (
        P("ep", None), P(), P(None, "tp"), P(), P(), P(), P(), P(), P(),
        P("ep", "tp", None, None), P("ep", "tp", None, None), P("ep", "tp", None), P("ep"),
        P("tp", None), P(), P(),
        P(None, ("ep", "tp")), P(None, ("ep", "tp")), P(("ep", "tp"), None),
        P("ep", None), P("ep", None),
        P("ep", None, "tp"), P("ep", None, "tp"), P("ep", "tp", None),
    )
    return jax.shard_map(
        body,
        mesh=mesh,
        in_specs=placed,
        out_specs=(P("ep", "tp"), P("ep", "tp", None), P("ep", "tp", None), P("ep", "tp")),
        check_vma=False,
    )
```

profile of v0, /device:TPU:0, one launch (start us, length us, event | category | flops | bytes accessed | tf_op | source)
XLA Modules:
  0.0 77.4 jit_solution(16379244251812877747)
XLA Ops:
  0.7 0.1 pad_add_fusion.ids
  0.7 0.7 copy-done.3
  1.4 0.0 copy-start.2
  1.4 9.4 %shard_map.255 = (bf16[24,2048]{1,0:T(8,128)(2,1)S(1)}, bf16[24,64]{1,0:T(8,128)(2,1)S(1)}, bf16[24,64]{1,0:T(8,128)(2,1)S(1)}, f32[24,8]{1,0:T(8,128)S(1)}) custom-call(s32[6]{0:T(128)S(1)} %pad_add_fusion.ids, s32[24]{0:T(128)S(1)} %copy-done.3, bf16[24,2048]{1,0:T(8,128)(2,1)} %tokens.1, bf16[2048]{0:T(1024)(128)(2,1)} %norm_in.1, bf16[64]{0:T(256)(128)(2,1)} %query_in.1, ...), custom_call_target="tpu_custom_call" | custom-call | tf_op jit(solution)/shard_map/pallas_call | solution.py:61
  10.9 0.6 collective-permute-start
  11.4 0.0 copy-done.4
  11.4 0.1 copy.52
  11.5 0.0 copy-done.5
  11.5 0.1 copy.55
  11.6 0.1 copy.54
  11.7 0.1 copy.53
  11.8 0.1 eq.17
  11.9 0.1 fusion
  12.0 0.1 reduce_sum.12
  12.2 0.1 fusion.5.notes.refs_7_
  12.2 0.1 collective-permute-done.part_b
  12.4 0.0 copy-done
  12.4 0.0 copy-done.1
  12.4 0.8 %shard_map.256 = (bf16[24,1152]{1,0:T(8,128)(2,1)S(1)}, bf16[24,1024]{1,0:T(8,128)(2,1)S(1)}, f32[24,128]{1,0:T(8,128)S(1)}) custom-call(s32[6]{0:T(128)S(1)} %pad_add_fusion.ids, bf16[24,2048]{1,0:T(8,128)(2,1)S(1)} %copy-done, bf16[24,2048]{1,0:T(8,128)(2,1)S(1)} %get-tuple-element.29.part_a, bf16[24,2048]{1,0:T(8,128)(2,1)S(1)} %collective-permute-done.part_b, ...), custom_call_target="tpu_custom_call" | custom-call | tf_op jit(solution)/shard_map/pallas_call | solution.py:61
  13.2 5.0 %collective-permute-start.3 = (bf16[24,1152]{1,0:T(8,128)(2,1)S(1)}, bf16[24,1152]{1,0:T(8,128)(2,1)S(1)}, u32[]{:S(2)}, u32[]{:S(2)}) collective-permute-start(bf16[24,1152]{1,0:T(8,128)(2,1)S(1)} %get-tuple-element.30), channel_id=1, source_target_pairs={{0,24},{2,26},{4,28},{6,30},{8,16},{10,18},{12,20},{14,22},{16,8},... | collective-permute-start | bytes 165896 | tf_op jit(solution)/shard_map/ppermute | solution.py:464
  18.2 0.0 collective-permute-start.2
  18.2 0.6 collective-permute-start.1
  18.8 3.5 %collective-permute-done.1 = bf16[24,1152]{1,0:T(8,128)(2,1)S(1)} collective-permute-done((bf16[24,1152]{1,0:T(8,128)(2,1)S(1)}, bf16[24,1152]{1,0:T(8,128)(2,1)S(1)}, u32[]{:S(2)}, u32[]{:S(2)}) %collective-permute-start.1) | collective-permute-done | bytes 55328 | tf_op jit(solution)/shard_map/ppermute | solution.py:464
  22.4 1.0 %collective-permute-done.2 = bf16[24,1152]{1,0:T(8,128)(2,1)S(1)} collective-permute-done((bf16[24,1152]{1,0:T(8,128)(2,1)S(1)}, bf16[24,1152]{1,0:T(8,128)(2,1)S(1)}, u32[]{:S(2)}, u32[]{:S(2)}) %collective-permute-start.2) | collective-permute-done | bytes 55328 | tf_op jit(solution)/shard_map/ppermute | solution.py:464
  23.3 0.0 collective-permute-done.3
  23.4 5.3 %shard_map.257 = (bf16[4,64,24]{2,1,0:T(8,128)(2,1)S(1)}, bf16[2048,512]{1,0:T(8,128)(2,1)S(1)}, bf16[2048,512]{1,0:T(8,128)(2,1)S(1)}, bf16[2048,512]{1,0:T(8,1...) custom-call(s32[6]{0:T(128)S(1)} %pad_add_fusion.ids, ...), custom_call_target="tpu_custom_call" | custom-call | tf_op jit(solution)/shard_map/pallas_call | solution.py:61
  28.7 0.1 collective-permute-start.12
  28.8 2.5 %collective-permute-start.6 = (bf16[96,1152]{1,0:T(8,128)(2,1)S(1)}, bf16[96,1152]{1,0:T(8,128)(2,1)S(1)}, u32[]{:S(2)}, u32[]{:S(2)}) collective-permute-start(bf16[96,1152]{1,0:T(8,128)(2,1)S(1)} %constant_dynamic-update-slice_fusion.column.refs_0_), channel_id=1, source_target_pairs={{0,6},{2,4},{4,2},{6,0},{8,14},{10,12},{12,10},{14,8},{16,22},{18,... | collective-permute-start | bytes 663560 | tf_op jit(solution)/shard_map/ppermute | solution.py:464
  31.3 0.5 collective-permute-start.5
  31.8 0.5 collective-permute-start.4
  32.3 0.0 collective-permute-start.7
  32.3 5.8 %collective-permute-done.6.refs_3_ = bf16[96,1152]{1,0:T(8,128)(2,1)S(1)} collective-permute-done((bf16[96,1152]{1,0:T(8,128)(2,1)S(1)}, bf16[96,1152]{1,0:T(8,128)(2,1)S(1)}, u32[]{:S(2)}, u32[]{:S(2)}) %collective-permute-start.6) | collective-permute-done | bytes 221216 | tf_op jit(solution)/shard_map/ppermute | solution.py:464
  38.1 0.0 collective-permute-start.10
  38.1 4.2 %collective-permute-done.5.refs_2_ = bf16[96,1152]{1,0:T(8,128)(2,1)S(1)} collective-permute-done((bf16[96,1152]{1,0:T(8,128)(2,1)S(1)}, bf16[96,1152]{1,0:T(8,128)(2,1)S(1)}, u32[]{:S(2)}, u32[]{:S(2)}) %collective-permute-start.5) | collective-permute-done | bytes 221216 | tf_op jit(solution)/shard_map/ppermute | solution.py:464
  42.2 0.0 collective-permute-start.9
  42.3 0.1 collective-permute-done.4.refs_1_
  42.3 0.4 collective-permute-start.8
  42.7 0.0 collective-permute-done.7.refs_4_
  42.7 0.0 collective-permute-done.10.refs_7_
  42.7 1.0 %collective-permute-done.9.refs_6_ = bf16[96,1152]{1,0:T(8,128)(2,1)S(1)} collective-permute-done((bf16[96,1152]{1,0:T(8,128)(2,1)S(1)}, bf16[96,1152]{1,0:T(8,128)(2,1)S(1)}, u32[]{:S(2)}, u32[]{:S(2)}) %collective-permute-start.9) | collective-permute-done | bytes 221216 | tf_op jit(solution)/shard_map/ppermute | solution.py:461
  43.7 0.3 collective-permute-done.8.refs_5_
  44.0 3.4 %shard_map.258 = (bf16[488,512]{1,0:T(8,128)(2,1)S(1)}, f32[96,128]{1,0:T(8,128)S(1)}) custom-call(s32[6]{0:T(128)S(1)} %pad_add_fusion.ids, bf16[96,1152]{1,0:T(8,128)(2,1)S(1)} %constant_dynamic-update-slice_fusion.column.refs_0_, bf16[96,1152]{1,0:T(8,128)(2,1)S(1)} %collective-permute-done.4.refs_1_, ...), custom_call_target="tpu_custom_call" | custom-call | tf_op jit(solution)/shard_map/pallas_call | solution.py:61
  47.4 0.3 collective-permute-start.11
  47.7 1.7 %collective-permute-done.11.other = bf16[488,512]{1,0:T(8,128)(2,1)S(1)} collective-permute-done((bf16[488,512]{1,0:T(8,128)(2,1)S(1)}, bf16[488,512]{1,0:T(8,128)(2,1)S(1)}, u32[]{:S(2)}, u32[]{:S(2)}) %collective-permute-start.11) | collective-permute-done | bytes 499744 | tf_op jit(solution)/shard_map/ppermute | solution.py:461
  49.3 0.0 collective-permute-done.12.down_got
  49.3 1.3 %shard_map.259 = (bf16[128,1024]{1,0:T(8,128)(2,1)S(1)}, bf16[128,1024]{1,0:T(8,128)(2,1)S(1)}, bf16[128,1024]{1,0:T(8,128)(2,1)S(1)}, bf16[128,1024]{1,0:T(8,128)(2,1)S(1)}) custom-call(bf16[488,512]{1,0:T(8,128)(2,1)S(1)} %get-tuple-element.35.own, bf16[488,512]{1,0:T(8,128)(2,1)S(1)} %collective-permute-done.11.other, ...), custom_call_target="tpu_custom_call" | custom-call | tf_op jit(solution)/shard_map/pallas_call | solution.py:61
  50.7 1.5 %collective-permute-start.13 = (bf16[128,1024]{1,0:T(8,128)(2,1)S(1)}, bf16[128,1024]{1,0:T(8,128)(2,1)S(1)}, u32[]{:S(2)}, u32[]{:S(2)}) collective-permute-start(bf16[128,1024]{1,0:T(8,128)(2,1)S(1)} %get-tuple-element.41), channel_id=1, source_target_pairs={{0,2},{2,0},{4,6},{6,4},{8,10},{10,8},{12,14},{14,12},{16,18},{18,... | collective-permute-start | bytes 786440 | tf_op jit(solution)/shard_map/ppermute | solution.py:464
  52.2 0.8 %collective-permute-start.14 = (bf16[128,1024]{1,0:T(8,128)(2,1)S(1)}, bf16[128,1024]{1,0:T(8,128)(2,1)S(1)}, u32[]{:S(2)}, u32[]{:S(2)}) collective-permute-start(bf16[128,1024]{1,0:T(8,128)(2,1)S(1)} %get-tuple-element.42), channel_id=1, source_target_pairs={{0,4},{2,6},{4,0},{6,2},{8,12},{10,14},{12,8},{14,10},{16,20},{18,... | collective-permute-start | bytes 786440 | tf_op jit(solution)/shard_map/ppermute | solution.py:464
  53.0 1.2 %collective-permute-start.15 = (bf16[128,1024]{1,0:T(8,128)(2,1)S(1)}, bf16[128,1024]{1,0:T(8,128)(2,1)S(1)}, u32[]{:S(2)}, u32[]{:S(2)}) collective-permute-start(bf16[128,1024]{1,0:T(8,128)(2,1)S(1)} %get-tuple-element.43), channel_id=1, source_target_pairs={{0,6},{2,4},{4,2},{6,0},{8,14},{10,12},{12,10},{14,8},{16,22},{18,... | collective-permute-start | bytes 786440 | tf_op jit(solution)/shard_map/ppermute | solution.py:464
  54.2 0.6 copy.61
  54.8 0.6 copy.62
  55.4 0.7 copy.56
  56.1 3.8 %collective-permute-done.13.refs_1_ = bf16[128,1024]{1,0:T(8,128)(2,1)S(1)} collective-permute-done((bf16[128,1024]{1,0:T(8,128)(2,1)S(1)}, bf16[128,1024]{1,0:T(8,128)(2,1)S(1)}, u32[]{:S(2)}, u32[]{:S(2)}) %collective-permute-start.13) | collective-permute-done | bytes 262176 | tf_op jit(solution)/shard_map/ppermute | solution.py:464
  59.9 6.0 %collective-permute-done.14.refs_2_ = bf16[128,1024]{1,0:T(8,128)(2,1)S(1)} collective-permute-done((bf16[128,1024]{1,0:T(8,128)(2,1)S(1)}, bf16[128,1024]{1,0:T(8,128)(2,1)S(1)}, u32[]{:S(2)}, u32[]{:S(2)}) %collective-permute-start.14) | collective-permute-done | bytes 262176 | tf_op jit(solution)/shard_map/ppermute | solution.py:464
  65.9 0.0 collective-permute-done.15.refs_3_
  65.9 0.3 shard_map.260
  66.2 1.3 %collective-permute-start.16 = (bf16[40,1024]{1,0:T(8,128)(2,1)S(1)}, bf16[40,1024]{1,0:T(8,128)(2,1)S(1)}, u32[]{:S(2)}, u32[]{:S(2)}) collective-permute-start(bf16[40,1024]{1,0:T(8,128)(2,1)S(1)} %get-tuple-element.46), channel_id=1, source_target_pairs={{0,8},{2,10},{4,12},{6,14},{8,0},{10,2},{12,4},{14,6},{16,24},{18,... | collective-permute-start | bytes 245768 | tf_op jit(solution)/shard_map/ppermute | solution.py:464
  67.5 1.8 %collective-permute-start.17 = (bf16[40,1024]{1,0:T(8,128)(2,1)S(1)}, bf16[40,1024]{1,0:T(8,128)(2,1)S(1)}, u32[]{:S(2)}, u32[]{:S(2)}) collective-permute-start(bf16[40,1024]{1,0:T(8,128)(2,1)S(1)} %get-tuple-element.47), channel_id=1, source_target_pairs={{0,16},{2,18},{4,20},{6,22},{8,24},{10,26},{12,28},{14,30},{16,0},... | collective-permute-start | bytes 245768 | tf_op jit(solution)/shard_map/ppermute | solution.py:464
  69.3 1.4 %collective-permute-start.18 = (bf16[40,1024]{1,0:T(8,128)(2,1)S(1)}, bf16[40,1024]{1,0:T(8,128)(2,1)S(1)}, u32[]{:S(2)}, u32[]{:S(2)}) collective-permute-start(bf16[40,1024]{1,0:T(8,128)(2,1)S(1)} %get-tuple-element.48), channel_id=1, source_target_pairs={{0,24},{2,26},{4,28},{6,30},{8,16},{10,18},{12,20},{14,22},{16,8},... | collective-permute-start | bytes 245768 | tf_op jit(solution)/shard_map/ppermute | solution.py:464
  70.7 0.6 collective-permute-done.16.refs_2_
  71.3 4.7 %collective-permute-done.17.refs_3_ = bf16[40,1024]{1,0:T(8,128)(2,1)S(1)} collective-permute-done((bf16[40,1024]{1,0:T(8,128)(2,1)S(1)}, bf16[40,1024]{1,0:T(8,128)(2,1)S(1)}, u32[]{:S(2)}, u32[]{:S(2)}) %collective-permute-start.17) | collective-permute-done | bytes 81952 | tf_op jit(solution)/shard_map/ppermute | solution.py:464
  76.0 0.0 collective-permute-done.18.refs_4_
  76.0 0.8 %shard_map.261 = bf16[24,1024]{1,0:T(8,128)(2,1)S(1)} custom-call(s32[4]{0:T(128)S(1)} %iota_xor_fusion.refs_0_, bf16[40,1024]{1,0:T(8,128)(2,1)S(1)} %get-tuple-element.45.refs_1_, bf16[40,1024]{1,0:T(8,128)(2,1)S(1)} %collective-permute-done.16.refs_2_, bf16[40,1024]{1,0:T(8,128)(2,1)S(1)} %collective-permute-done.17.refs_3_, ...), custom_call_target="tpu_custom_call" | custom-call | tf_op jit(solution)/shard_map/pallas_call | solution.py:61
  76.8 0.6 copy.60
  (15 shorter events, 0.1 us)
Async XLA Ops:
  0.7 0.7 copy-start.3
  1.4 10.0 %copy-start.4 = (s32[24,2]{0,1:T(2,128)S(1)}, s32[24,2]{0,1:T(2,128)}, u32[]{:S(2)}) copy-start(s32[24,2]{0,1:T(2,128)} %param.43) | copy-start | bytes 580
  1.4 10.1 %copy-start.5 = (f32[24,2]{0,1:T(2,128)S(1)}, f32[24,2]{0,1:T(2,128)}, u32[]{:S(2)}) copy-start(f32[24,2]{0,1:T(2,128)} %param.44) | copy-start | bytes 580
  1.4 11.0 %copy-start = (bf16[24,2048]{1,0:T(8,128)(2,1)S(1)}, bf16[24,2048]{1,0:T(8,128)(2,1)}, u32[]{:S(2)}) copy-start(bf16[24,2048]{1,0:T(8,128)(2,1)} %tokens.1) | copy-start | bytes 294916
  1.4 11.0 %copy-start.1 = (bf16[2048]{0:T(1024)(128)(2,1)S(1)}, bf16[2048]{0:T(1024)(128)(2,1)}, u32[]{:S(2)}) copy-start(bf16[2048]{0:T(1024)(128)(2,1)} %gain.1) | copy-start | bytes 12292
  1.4 11.0 %copy-start.2 = (bf16[2048]{0:T(1024)(128)(2,1)S(1)}, bf16[2048]{0:T(1024)(128)(2,1)}, u32[]{:S(2)}) copy-start(bf16[2048]{0:T(1024)(128)(2,1)} %branch_gate.1) | copy-start | bytes 12292
  10.9 1.5 %collective-permute-start = (bf16[24,2048]{1,0:T(8,128)(2,1)S(1)}, bf16[24,2048]{1,0:T(8,128)(2,1)S(1)}, u32[]{:S(2)}, u32[]{:S(2)}) collective-permute-start(bf16[24,2048]{1,0:T(8,128)(2,1)S(1)} %get-tuple-element.29.part_a), channel_id=1, source_target_pairs={{0,1},{1,0},{2,3},{3,2},{4,5},{5,4},{6,7},{7,6},{8,9},{9,8},{10,11... | collective-permute-start | bytes 294920 | tf_op jit(solution)/shard_map/ppermute | solution.py:461
  13.2 10.2 %collective-permute-start.3 = (bf16[24,1152]{1,0:T(8,128)(2,1)S(1)}, bf16[24,1152]{1,0:T(8,128)(2,1)S(1)}, u32[]{:S(2)}, u32[]{:S(2)}) collective-permute-start(bf16[24,1152]{1,0:T(8,128)(2,1)S(1)} %get-tuple-element.30), channel_id=1, source_target_pairs={{0,24},{2,26},{4,28},{6,30},{8,16},{10,18},{12,20},{14,22},{16,8},... | collective-permute-start | bytes 165896 | tf_op jit(solution)/shard_map/ppermute | solution.py:464
  18.2 5.2 %collective-permute-start.2 = (bf16[24,1152]{1,0:T(8,128)(2,1)S(1)}, bf16[24,1152]{1,0:T(8,128)(2,1)S(1)}, u32[]{:S(2)}, u32[]{:S(2)}) collective-permute-start(bf16[24,1152]{1,0:T(8,128)(2,1)S(1)} %get-tuple-element.30), channel_id=1, source_target_pairs={{0,16},{2,18},{4,20},{6,22},{8,24},{10,26},{12,28},{14,30},{16,0},... | collective-permute-start | bytes 165896 | tf_op jit(solution)/shard_map/ppermute | solution.py:464
  18.2 4.2 %collective-permute-start.1 = (bf16[24,1152]{1,0:T(8,128)(2,1)S(1)}, bf16[24,1152]{1,0:T(8,128)(2,1)S(1)}, u32[]{:S(2)}, u32[]{:S(2)}) collective-permute-start(bf16[24,1152]{1,0:T(8,128)(2,1)S(1)} %get-tuple-element.30), channel_id=1, source_target_pairs={{0,8},{2,10},{4,12},{6,14},{8,0},{10,2},{12,4},{14,6},{16,24},{18,... | collective-permute-start | bytes 165896 | tf_op jit(solution)/shard_map/ppermute | solution.py:464
  28.7 20.7 %collective-permute-start.12 = (bf16[1024,1024]{1,0:T(8,128)(2,1)S(1)}, bf16[1024,1024]{1,0:T(8,128)(2,1)S(1)}, u32[]{:S(2)}, u32[]{:S(2)}) collective-permute-start(bf16[1024,1024]{1,0:T(8,128)(2,1)S(1)} %get-tuple-element.38), channel_id=1, source_target_pairs={{0,1},{1,0},{2,3},{3,2},{4,5},{5,4},{6,7},{7,6},{8,9},{9,8},{10,11... | collective-permute-start | bytes 6291464 | tf_op jit(solution)/shard_map/ppermute | solution.py:461
  28.8 9.3 %collective-permute-start.6 = (bf16[96,1152]{1,0:T(8,128)(2,1)S(1)}, bf16[96,1152]{1,0:T(8,128)(2,1)S(1)}, u32[]{:S(2)}, u32[]{:S(2)}) collective-permute-start(bf16[96,1152]{1,0:T(8,128)(2,1)S(1)} %constant_dynamic-update-slice_fusion.column.refs_0_), channel_id=1, source_target_pairs={{0,6},{2,4},{4,2},{6,0},{8,14},{10,12},{12,10},{14,8},{16,22},{18,... | collective-permute-start | bytes 663560 | tf_op jit(solution)/shard_map/ppermute | solution.py:464
  31.3 11.0 %collective-permute-start.5 = (bf16[96,1152]{1,0:T(8,128)(2,1)S(1)}, bf16[96,1152]{1,0:T(8,128)(2,1)S(1)}, u32[]{:S(2)}, u32[]{:S(2)}) collective-permute-start(bf16[96,1152]{1,0:T(8,128)(2,1)S(1)} %constant_dynamic-update-slice_fusion.column.refs_0_), channel_id=1, source_target_pairs={{0,4},{2,6},{4,0},{6,2},{8,12},{10,14},{12,8},{14,10},{16,20},{18,... | collective-permute-start | bytes 663560 | tf_op jit(solution)/shard_map/ppermute | solution.py:464
  31.8 10.6 %collective-permute-start.4 = (bf16[96,1152]{1,0:T(8,128)(2,1)S(1)}, bf16[96,1152]{1,0:T(8,128)(2,1)S(1)}, u32[]{:S(2)}, u32[]{:S(2)}) collective-permute-start(bf16[96,1152]{1,0:T(8,128)(2,1)S(1)} %constant_dynamic-update-slice_fusion.column.refs_0_), channel_id=1, source_target_pairs={{0,2},{2,0},{4,6},{6,4},{8,10},{10,8},{12,14},{14,12},{16,18},{18,... | collective-permute-start | bytes 663560 | tf_op jit(solution)/shard_map/ppermute | solution.py:464
  32.3 10.4 %collective-permute-start.7 = (bf16[96,1152]{1,0:T(8,128)(2,1)S(1)}, bf16[96,1152]{1,0:T(8,128)(2,1)S(1)}, u32[]{:S(2)}, u32[]{:S(2)}) collective-permute-start(bf16[96,1152]{1,0:T(8,128)(2,1)S(1)} %constant_dynamic-update-slice_fusion.column.refs_0_), channel_id=1, source_target_pairs={{0,1},{1,0},{2,3},{3,2},{4,5},{5,4},{6,7},{7,6},{8,9},{9,8},{10,11... | collective-permute-start | bytes 663560 | tf_op jit(solution)/shard_map/ppermute | solution.py:461
  38.1 4.7 %collective-permute-start.10 = (bf16[96,1152]{1,0:T(8,128)(2,1)S(1)}, bf16[96,1152]{1,0:T(8,128)(2,1)S(1)}, u32[]{:S(2)}, u32[]{:S(2)}) collective-permute-start(bf16[96,1152]{1,0:T(8,128)(2,1)S(1)} %collective-permute-done.6.refs_3_), channel_id=1, source_target_pairs={{0,1},{1,0},{2,3},{3,2},{4,5},{5,4},{6,7},{7,6},{8,9},{9,8},{10,11... | collective-permute-start | bytes 663560 | tf_op jit(solution)/shard_map/ppermute | solution.py:461
  42.2 1.5 %collective-permute-start.9 = (bf16[96,1152]{1,0:T(8,128)(2,1)S(1)}, bf16[96,1152]{1,0:T(8,128)(2,1)S(1)}, u32[]{:S(2)}, u32[]{:S(2)}) collective-permute-start(bf16[96,1152]{1,0:T(8,128)(2,1)S(1)} %collective-permute-done.5.refs_2_), channel_id=1, source_target_pairs={{0,1},{1,0},{2,3},{3,2},{4,5},{5,4},{6,7},{7,6},{8,9},{9,8},{10,11... | collective-permute-start | bytes 663560 | tf_op jit(solution)/shard_map/ppermute | solution.py:461
  42.3 1.7 %collective-permute-start.8 = (bf16[96,1152]{1,0:T(8,128)(2,1)S(1)}, bf16[96,1152]{1,0:T(8,128)(2,1)S(1)}, u32[]{:S(2)}, u32[]{:S(2)}) collective-permute-start(bf16[96,1152]{1,0:T(8,128)(2,1)S(1)} %collective-permute-done.4.refs_1_), channel_id=1, source_target_pairs={{0,1},{1,0},{2,3},{3,2},{4,5},{5,4},{6,7},{7,6},{8,9},{9,8},{10,11... | collective-permute-start | bytes 663560 | tf_op jit(solution)/shard_map/ppermute | solution.py:461
  47.4 1.9 %collective-permute-start.11 = (bf16[488,512]{1,0:T(8,128)(2,1)S(1)}, bf16[488,512]{1,0:T(8,128)(2,1)S(1)}, u32[]{:S(2)}, u32[]{:S(2)}) collective-permute-start(bf16[488,512]{1,0:T(8,128)(2,1)S(1)} %get-tuple-element.35.own), channel_id=1, source_target_pairs={{0,1},{1,0},{2,3},{3,2},{4,5},{5,4},{6,7},{7,6},{8,9},{9,8},{10,11... | collective-permute-start | bytes 1499144 | tf_op jit(solution)/shard_map/ppermute | solution.py:461
  50.7 9.2 %collective-permute-start.13 = (bf16[128,1024]{1,0:T(8,128)(2,1)S(1)}, bf16[128,1024]{1,0:T(8,128)(2,1)S(1)}, u32[]{:S(2)}, u32[]{:S(2)}) collective-permute-start(bf16[128,1024]{1,0:T(8,128)(2,1)S(1)} %get-tuple-element.41), channel_id=1, source_target_pairs={{0,2},{2,0},{4,6},{6,4},{8,10},{10,8},{12,14},{14,12},{16,18},{18,... | collective-permute-start | bytes 786440 | tf_op jit(solution)/shard_map/ppermute | solution.py:464
  52.2 13.7 %collective-permute-start.14 = (bf16[128,1024]{1,0:T(8,128)(2,1)S(1)}, bf16[128,1024]{1,0:T(8,128)(2,1)S(1)}, u32[]{:S(2)}, u32[]{:S(2)}) collective-permute-start(bf16[128,1024]{1,0:T(8,128)(2,1)S(1)} %get-tuple-element.42), channel_id=1, source_target_pairs={{0,4},{2,6},{4,0},{6,2},{8,12},{10,14},{12,8},{14,10},{16,20},{18,... | collective-permute-start | bytes 786440 | tf_op jit(solution)/shard_map/ppermute | solution.py:464
  53.0 12.9 %collective-permute-start.15 = (bf16[128,1024]{1,0:T(8,128)(2,1)S(1)}, bf16[128,1024]{1,0:T(8,128)(2,1)S(1)}, u32[]{:S(2)}, u32[]{:S(2)}) collective-permute-start(bf16[128,1024]{1,0:T(8,128)(2,1)S(1)} %get-tuple-element.43), channel_id=1, source_target_pairs={{0,6},{2,4},{4,2},{6,0},{8,14},{10,12},{12,10},{14,8},{16,22},{18,... | collective-permute-start | bytes 786440 | tf_op jit(solution)/shard_map/ppermute | solution.py:464
  66.2 5.1 %collective-permute-start.16 = (bf16[40,1024]{1,0:T(8,128)(2,1)S(1)}, bf16[40,1024]{1,0:T(8,128)(2,1)S(1)}, u32[]{:S(2)}, u32[]{:S(2)}) collective-permute-start(bf16[40,1024]{1,0:T(8,128)(2,1)S(1)} %get-tuple-element.46), channel_id=1, source_target_pairs={{0,8},{2,10},{4,12},{6,14},{8,0},{10,2},{12,4},{14,6},{16,24},{18,... | collective-permute-start | bytes 245768 | tf_op jit(solution)/shard_map/ppermute | solution.py:464
  67.5 8.5 %collective-permute-start.17 = (bf16[40,1024]{1,0:T(8,128)(2,1)S(1)}, bf16[40,1024]{1,0:T(8,128)(2,1)S(1)}, u32[]{:S(2)}, u32[]{:S(2)}) collective-permute-start(bf16[40,1024]{1,0:T(8,128)(2,1)S(1)} %get-tuple-element.47), channel_id=1, source_target_pairs={{0,16},{2,18},{4,20},{6,22},{8,24},{10,26},{12,28},{14,30},{16,0},... | collective-permute-start | bytes 245768 | tf_op jit(solution)/shard_map/ppermute | solution.py:464
  69.3 6.7 %collective-permute-start.18 = (bf16[40,1024]{1,0:T(8,128)(2,1)S(1)}, bf16[40,1024]{1,0:T(8,128)(2,1)S(1)}, u32[]{:S(2)}, u32[]{:S(2)}) collective-permute-start(bf16[40,1024]{1,0:T(8,128)(2,1)S(1)} %get-tuple-element.48), channel_id=1, source_target_pairs={{0,24},{2,26},{4,28},{6,30},{8,16},{10,18},{12,20},{14,22},{16,8},... | collective-permute-start | bytes 245768 | tf_op jit(solution)/shard_map/ppermute | solution.py:464
where the time goes:
time: 77.6 us; the launch traced here: 77.4 us
  waiting for transfers between devices  32.7 us (42%)
  Pallas kernels  21.3 us (27%)
  starting transfers between devices  18.6 us (24%)
  local copies, waits for them, and re-layouts  3.75 us (5%)
  between operations  0.78 us (1%)
    ppermute x12, waiting for transfers between devices, exchange(): return lax.ppermute(values, 'ep', [(i, i ^ mask) for i in range(ep_count)])  29.7 us
    pallas_call x7, Pallas kernels, call(): pl.pallas_call(kernel, in_specs=specs, out_specs=[VMEM] * len(outs), out_...  21.3 us
    ppermute x12, starting transfers between devices, exchange(): return lax.ppermute(values, 'ep', [(i, i ^ mask) for i in range(ep_count)])  17.2 us
    unnamed x20, local copies, waits for them, and re-layouts  3.26 us
    ppermute x7, waiting for transfers between devices, swap(): return lax.ppermute(values, 'tp', [(i, 1 - i) for i in range(tp_count)])  3.07 us
  transfers between devices with their start and end apart: 19, of which 13 were waited for; matrix products, arithmetic and copies ran while one was open for 3% of the time, Pallas kernels for 4%

commit v1 on v0

--- a/solution.py
+++ b/solution.py
@@ -111,9 +111,19 @@
     resid[...] = jnp.where(first, total[:, :half], total[:, half:]).astype(BF16)
 
 
+def fetch_kernel(anchor, *refs):
+    count = (len(refs) - 1) // 2
+    copies = [
+        pltpu.make_async_copy(refs[i], refs[count + i], refs[-1].at[i]) for i in range(count)
+    ]
+    for copy in copies:
+        copy.start()
+    for copy in copies:
+        copy.wait()
+
+
 def load_kernel(
-    ids, column, gate_in, up_in, expert_gate_in, expert_up_in, down_in, expert_in,
-    combine, gate_w, up_w, expert_gate, expert_up, down_own, expert_own, down_sent, sems,
+    ids, column, down_in, expert_in, combine, down_own, expert_own, down_sent, sems,
     *, seq, capacity, top_k,
 ):
     hidden, half = down_own.shape
@@ -123,8 +133,7 @@
     pairs = [
         (down_in.at[:, theirs], down_sent.at[pl.ds(0, hidden)]),
         (expert_in.at[:, theirs], down_sent.at[pl.ds(hidden, other)]),
-        (gate_in, gate_w), (up_in, up_w), (expert_gate_in, expert_gate),
-        (expert_up_in, expert_up), (down_in.at[:, mine], down_own),
+        (down_in.at[:, mine], down_own),
         (expert_in.at[:, mine], expert_own),
     ]
     copies = [pltpu.make_async_copy(a, b, sems.at[i]) for i, (a, b) in enumerate(pairs)]
@@ -178,12 +187,13 @@
     hidden = silu(project(left, right, gate_w)) * project(left, right, up_w)
     out[0:count, 0 : gate_w.shape[1]] = hidden.astype(BF16)
     squares = jnp.sum(hidden * hidden, axis=1, keepdims=True)
-    tile_row = lax.broadcasted_iota(jnp.int32, (2 * plane, LANES), 0)
-    tile = jnp.zeros((2 * plane, LANES), F32)
+    extra = out.shape[0] - count - slots
+    tile_row = lax.broadcasted_iota(jnp.int32, (extra, LANES), 0)
+    tile = jnp.zeros((extra, LANES), F32)
     for j in range(plane):
         high, low = high_low(to_row(squares[j * group : (j + 1) * group]))
         tile = jnp.where(tile_row == 2 * j, high, jnp.where(tile_row == 2 * j + 1, low, tile))
-    out[count + slots :, :] = jnp.zeros((2 * plane, out.shape[1]), BF16)
+    out[count + slots :, :] = jnp.zeros((extra, out.shape[1]), BF16)
     out[count + slots :, 0:LANES] = tile.astype(BF16)
 
     turned = jnp.transpose(notes[...])
@@ -292,11 +302,11 @@
 
 
 def attend_kernel(
-    ids, lens, tokens_in, norm_in, query_in, key_in, bias_in,
+    ids, lens_in, tokens_in, norm_in, query_in, key_in, bias_in,
     query_w, key_w, value_w, forget_w, cache_key, cache_value, cache_gate, out_w,
     partial, fresh_key, fresh_value, fresh_gate,
     q_w, k_w, v_w, f_w, keys, values, gates, o_w, q_rows, k_rows, v_rows, f_cols, g_cols, mixed,
-    tokens, norm_gain, query_gain, key_gain, forget_bias, sems,
+    tokens, norm_gain, query_gain, key_gain, forget_bias, lens, sems,
     *, heads, chunks,
 ):
     seq = tokens.shape[0]
@@ -305,7 +315,7 @@
     step = seq // chunks
     plain = [
         (tokens_in, tokens), (norm_in, norm_gain), (query_in, query_gain), (key_in, key_gain),
-        (bias_in, forget_bias), (key_w, k_w), (value_w, v_w), (forget_w, f_w), (query_w, q_w),
+        (bias_in, forget_bias), (lens_in, lens), (key_w, k_w), (value_w, v_w), (forget_w, f_w), (query_w, q_w),
     ]
     small = [pltpu.make_async_copy(a, b, sems.at[i]) for i, (a, b) in enumerate(plain)]
     base = len(small)
@@ -317,9 +327,9 @@
     last = pltpu.make_async_copy(out_w, o_w, sems.at[base + len(parts)])
     for copy in small + parts + [last]:
         copy.start()
-    for copy in small[:5]:
+    for copy in small[:6]:
         copy.wait()
-    small = small[5:]
+    small = small[6:]
     first = ids[0] == 0
     resid = tokens[...].astype(F32)
     mean_square = jnp.mean(resid * resid, axis=-1, keepdims=True)
@@ -347,47 +357,63 @@
     f_cols[...] = jnp.transpose(wide)[0:heads]
     small[3].wait()
     queries = dot(normed, q_w[...])
+    scale = head ** (-0.5)
     for h in range(heads):
         part = queries[:, h * head : (h + 1) * head]
         part = rms_scale(part, query_gain[...].astype(F32)[None]).astype(BF16)
-        q_rows[:, h, :] = part.astype(F32)
+        q_rows[:, h, :] = part.astype(F32) * scale
     g_cols[...] = jnp.zeros(g_cols.shape, F32)
     lane = lax.broadcasted_iota(jnp.int32, (heads, span), 1)
     lane_small = lax.broadcasted_iota(jnp.int32, (heads, LANES), 1)
-    scale = head ** (-0.5)
-
-    def one(s):
-        length = lens[s]
-        place = length - 1
-        block = pl.multiple_of((place // LANES) * LANES, LANES)
-        near = gates[s, :, pl.ds(block, LANES)]
-        previous = jnp.sum(
-            jnp.where(lane_small == place - block, near, 0.0), axis=1, keepdims=True
-        )
-        log_forget = f_cols[:, s : s + 1]
-        current = previous + log_forget
-        g_cols[:, s : s + 1] = current
-        query = q_rows[s]
-        own = jnp.sum(query * k_rows[s : s + 1], axis=1, keepdims=True) * scale
-        logits = dot(query.astype(BF16), keys[s]) * scale + (current - gates[s])
-        logits = jnp.where(lane < length, logits, -1e30)
-        top = jnp.maximum(jnp.max(logits, axis=1, keepdims=True), own)
-        weight = jnp.exp(logits - top)
-        own_weight = jnp.exp(own - top)
-        total = jnp.sum(weight, axis=1, keepdims=True) + own_weight
-        inverse = 1.0 / total
-        probs = (weight * inverse).astype(BF16)
-        own_prob = (own_weight * inverse).astype(BF16).astype(F32)
-        out = lax.dot_general(
-            probs, values[s], (((1,), (1,)), ((), ())), preferred_element_type=F32
-        )
-        mixed[s] = out + own_prob * v_rows[s : s + 1]
+
+    def several(span_of):
+        lengths = [lens[s] for s in span_of]
+        place = [length - 1 for length in lengths]
+        block = [pl.multiple_of((at // LANES) * LANES, LANES) for at in place]
+        near = [gates[s, :, pl.ds(at, LANES)] for s, at in zip(span_of, block)]
+        previous = [
+            jnp.sum(jnp.where(lane_small == at - start, value, 0.0), axis=1, keepdims=True)
+            for at, start, value in zip(place, block, near)
+        ]
+        current = [f_cols[:, s : s + 1] + value for s, value in zip(span_of, previous)]
+        for s, value in zip(span_of, current):
+            g_cols[:, s : s + 1] = value
+        query = [q_rows[s] for s in span_of]
+        scores = [dot(value.astype(BF16), keys[s]) for s, value in zip(span_of, query)]
+        own = [
+            jnp.sum(value * k_rows[s : s + 1], axis=1, keepdims=True)
+            for s, value in zip(span_of, query)
+        ]
+        logits = [
+            jnp.where(lane < length, score + (now - gates[s]), -1e30)
+            for s, length, score, now in zip(span_of, lengths, scores, current)
+        ]
+        top = [
+            jnp.maximum(jnp.max(value, axis=1, keepdims=True), mine)
+            for value, mine in zip(logits, own)
+        ]
+        weight = [jnp.exp(value - peak) for value, peak in zip(logits, top)]
+        own_weight = [jnp.exp(mine - peak) for mine, peak in zip(own, top)]
+        inverse = [
+            1.0 / (jnp.sum(value, axis=1, keepdims=True) + mine)
+            for value, mine in zip(weight, own_weight)
+        ]
+        probs = [(value * factor).astype(BF16) for value, factor in zip(weight, inverse)]
+        out = [
+            lax.dot_general(
+                value, values[s], (((1,), (1,)), ((), ())), preferred_element_type=F32
+            )
+            for s, value in zip(span_of, probs)
+        ]
+        for s, value, mine, factor in zip(span_of, out, own_weight, inverse):
+            own_prob = (mine * factor).astype(BF16).astype(F32)
+            mixed[s] = value + own_prob * v_rows[s : s + 1]
 
     for c in range(chunks):
         for copy in parts[3 * c : 3 * c + 3]:
             copy.wait()
-        for s in range(c * step, (c + 1) * step):
-            one(s)
+        for start in range(c * step, (c + 1) * step, 12):
+            several(range(start, min(start + 12, (c + 1) * step)))
     turned = jnp.concatenate([g_cols[...], jnp.zeros((LANES - heads, LANES), F32)], axis=0)
     fresh_gate[...] = jnp.transpose(turned)[0:seq, 0:heads]
     last.wait()
@@ -404,7 +430,7 @@
     seq, width = tokens.shape
     heads = cache_gate.shape[1]
     head, span = cache_key.shape[2:]
-    chunks = 3 if seq % 3 == 0 else 1
+    chunks = 2 if seq % 2 == 0 else 1
     scratch = [
         pltpu.VMEM(query_w.shape, BF16), pltpu.VMEM(key_w.shape, BF16),
         pltpu.VMEM(value_w.shape, BF16), pltpu.VMEM(forget_w.shape[::-1], BF16),
@@ -415,8 +441,8 @@
         pltpu.VMEM((heads, LANES), F32), pltpu.VMEM((seq, heads, head), F32),
         pltpu.VMEM(tokens.shape, BF16), pltpu.VMEM(norm_gain.shape, BF16),
         pltpu.VMEM(query_gain.shape, BF16), pltpu.VMEM(key_gain.shape, BF16),
-        pltpu.VMEM(forget_bias.shape, F32),
-        pltpu.SemaphoreType.DMA((10 + 3 * chunks,)),
+        pltpu.VMEM(forget_bias.shape, F32), pltpu.SMEM(cache_len.shape, jnp.int32),
+        pltpu.SemaphoreType.DMA((11 + 3 * chunks,)),
     ]
     partial, fresh_key, fresh_value, current = call(
         functools.partial(attend_kernel, heads=heads, chunks=chunks),
@@ -425,7 +451,7 @@
             ids, cache_len, tokens, norm_gain, query_gain, key_gain, forget_bias, query_w, key_w, value_w, forget_w.T,
             cache_key[:, 0], cache_value[:, 0], cache_gate, out_w,
         ],
-        hbm=range(2, 15),
+        hbm=range(1, 15),
         scratch=scratch,
         limit=32,
     )
@@ -452,7 +478,6 @@
     expert_local = expert_gate_w.shape[2]
     widest = max(ff_local, expert_local)
     ff_total = ff_local * ep_count * tp_count
-    count, slots = ep_count * seq, ep_count * capacity
     pair_rows = 8 * ((seq // 2 + 2 + 7) // 8)
     z_rank = ep_rank // plane
     p_rank = ep_rank % plane
@@ -481,47 +506,63 @@
         [((seq, half + LANES), BF16), ((seq, half), BF16), ((seq, LANES), F32)],
         [ids, tokens, partial, swap(partial), post_gain, branch_gate, notes],
     )
-    column = jnp.concatenate(
-        [payload] + [exchange(payload, k * plane) for k in range(1, planes)], axis=0
-    )
+    near = []
+    for k in range(1, planes):
+        near.append(exchange(payload, k * plane))
+    wide = [dense_gate_w, dense_up_w, expert_gate_w[0], expert_up_w[0]]
+    gate_w, up_w, expert_gate, expert_up = call(
+        fetch_kernel,
+        [(value.shape, BF16) for value in wide],
+        [payload, *wide],
+        hbm=range(1, 5),
+        scratch=[pltpu.SemaphoreType.DMA((4,))],
+    )
+    column = jnp.concatenate([payload] + near, axis=0)
     owns = [column] + [None] * (plane - 1)
     for j in reversed(range(1, plane)):
         owns[j] = exchange(column, j)
-    combine, gate_w, up_w, expert_gate, expert_up, down_own, expert_own, down_sent = call(
+    combine, down_own, expert_own, down_sent = call(
         functools.partial(load_kernel, seq=seq, capacity=capacity, top_k=top_k),
-        [((plane, planes * pair_rows, planes * capacity), BF16)]
-        + [(dense_gate_w.shape, BF16)] * 2
-        + [(expert_gate_w.shape[1:], BF16)] * 2
-        + [((ff_local, half), BF16), ((expert_local, half), BF16)]
-        + [((ff_local + expert_local, half), BF16)],
         [
-            ids, column, dense_gate_w, dense_up_w, expert_gate_w[0], expert_up_w[0],
-            dense_down_w, expert_down_w[0],
+            ((plane, planes * pair_rows, planes * capacity), BF16),
+            ((ff_local, half), BF16),
+            ((expert_local, half), BF16),
+            ((ff_local + expert_local, half), BF16),
         ],
-        hbm=range(2, 8),
-        scratch=[pltpu.SemaphoreType.DMA((8,))],
+        [ids, column, dense_down_w, expert_down_w[0]],
+        hbm=range(2, 4),
+        scratch=[pltpu.SemaphoreType.DMA((4,))],
     )
     down_got = swap(down_sent)
-    others = [swap(values) for values in owns]
-    hidden, slot_weight = call(
-        functools.partial(hidden_kernel, seq=seq, capacity=capacity, top_k=top_k),
-        [((count + slots + 2 * plane, widest), BF16), ((slots, LANES), F32)],
-        [ids, *owns, *others, gate_w, up_w, expert_gate, expert_up],
-        scratch=[
-            pltpu.VMEM((count, half), BF16), pltpu.VMEM((count, half), BF16),
-            pltpu.VMEM((count, LANES), F32),
-        ],
-    )
-    sums = call(
-        functools.partial(down_kernel, count=count),
-        [((planes * (seq + capacity) + 8, half), BF16)] * plane,
-        [
-            hidden, swap(hidden), down_own, expert_own, down_got, slot_weight,
-        ],
-    )
-    arrived = [sums[0]] + [None] * (plane - 1)
-    for j in reversed(range(1, plane)):
-        arrived[j] = exchange(sums[j], j)
+    others = []
+    for j in range(plane):
+        others.append(swap(owns[j]))
+    arrived = [None] * plane
+    order = [0] + list(reversed(range(1, plane)))
+    for members in (order[: plane // 2], order[plane // 2 :]):
+        size = len(members)
+        rows, routes = size * planes * seq, size * planes * capacity
+        extra = 8 * ((2 * size + 7) // 8)
+        hidden, slot_weight = call(
+            functools.partial(hidden_kernel, seq=seq, capacity=capacity, top_k=top_k),
+            [((rows + routes + extra, widest), BF16), ((routes, LANES), F32)],
+            [
+                ids, *[owns[j] for j in members], *[others[j] for j in members],
+                gate_w, up_w, expert_gate, expert_up,
+            ],
+            scratch=[
+                pltpu.VMEM((rows, half), BF16), pltpu.VMEM((rows, half), BF16),
+                pltpu.VMEM((rows, LANES), F32),
+            ],
+        )
+        hidden_other = swap(hidden)
+        sums = call(
+            functools.partial(down_kernel, count=rows),
+            [((planes * (seq + capacity) + 8, half), BF16)] * size,
+            [hidden, hidden_other, down_own, expert_own, down_got, slot_weight],
+        )
+        for j, value in zip(members, sums):
+            arrived[j] = exchange(value, j) if j else value
     lasts = call(
         functools.partial(plane_kernel, planes=planes, seq=seq, capacity=capacity),
         [((seq + pair_rows, half), BF16)] * planes,

time: 77.6 us -> 74.2 us (0.956)
  waiting for transfers between devices: 32.7 us -> 29.2 us
    ppermute x7 -> x8, waiting for transfers between devices: 3.07 us -> 0.13 us  [swap(): return lax.ppermute(values, 'tp', [(i, 1 - i) for i in range(tp_count)])]
    unnamed x20 -> x18, local copies, waits for them, and re-layouts: 3.26 us -> 2.6 us
    ppermute x7 -> x8, starting transfers between devices: 1.35 us -> 1.76 us  [swap(): return lax.ppermute(values, 'tp', [(i, 1 - i) for i in range(tp_count)])]
    pallas_call x7 -> x10, Pallas kernels: 21.3 us -> 21.6 us  [call(): pl.pallas_call(kernel, in_specs=specs, out_specs=[VMEM] * len(outs), out_...]
  transfers between devices with their start and end apart: 19 -> 20, of which waited for: 13 -> 8; matrix products, arithmetic and copies ran while one was open for 3% -> 4% of each run, Pallas kernels for 4% -> 14%
where the time goes in v1:
time: 74.2 us; the launch traced here: 74.1 us
  waiting for transfers between devices  29.2 us (39%)
  Pallas kernels  21.6 us (29%)
  starting transfers between devices  19 us (26%)
  local copies, waits for them, and re-layouts  3.09 us (4%)
  between operations  0.84 us (1%)
    ppermute x12, waiting for transfers between devices, exchange(): return lax.ppermute(values, 'ep', [(i, i ^ mask) for i in range(ep_count)])  29 us
    pallas_call x10, Pallas kernels, call(): pl.pallas_call(kernel, in_specs=specs, out_specs=[VMEM] * len(outs), out_...  21.6 us
    ppermute x12, starting transfers between devices, exchange(): return lax.ppermute(values, 'ep', [(i, i ^ mask) for i in range(ep_count)])  17.3 us
    unnamed x18, local copies, waits for them, and re-layouts  2.6 us
    ppermute x8, starting transfers between devices, swap(): return lax.ppermute(values, 'tp', [(i, 1 - i) for i in range(tp_count)])  1.76 us
  transfers between devices with their start and end apart: 20, of which 8 were waited for; matrix products, arithmetic and copies ran while one was open for 4% of the time, Pallas kernels for 14%

profile of v1, /device:TPU:0, one launch (start us, length us, event | category | flops | bytes accessed | tf_op | source)
XLA Modules:
  0.0 74.1 jit_solution(17931334245079745512)
XLA Ops:
  0.7 0.1 pad_add_fusion.ids
  0.8 0.0 copy-start.2
  0.8 6.7 %shard_map.255 = (bf16[24,2048]{1,0:T(8,128)(2,1)S(1)}, bf16[24,64]{1,0:T(8,128)(2,1)S(1)}, bf16[24,64]{1,0:T(8,128)(2,1)S(1)}, f32[24,8]{1,0:T(8,128)S(1)}) custom-call(s32[6]{0:T(128)S(1)} %pad_add_fusion.ids, s32[24]{0:T(128)} %lens_in.1, bf16[24,2048]{1,0:T(8,128)(2,1)} %tokens.1, bf16[2048]{0:T(1024)(128)(2,1)} %norm_in.1, bf16[64]{0:T(256)(128)(2,1)} %query_in.1, ...), custom_call_target="tpu_custom_call" | custom-call | tf_op jit(solution)/shard_map/pallas_call | solution.py:61
  7.5 0.6 collective-permute-start
  8.1 0.1 copy.52
  8.1 0.1 copy.55
  8.2 0.1 copy.54
  8.3 0.1 copy.53
  8.4 0.1 eq.17
  8.5 0.1 fusion
  8.7 0.1 reduce_sum.12
  8.8 0.1 fusion.5.notes.refs_7_
  8.9 0.1 collective-permute-done.part_b
  9.0 0.8 %shard_map.256 = (bf16[24,1152]{1,0:T(8,128)(2,1)S(1)}, bf16[24,1024]{1,0:T(8,128)(2,1)S(1)}, f32[24,128]{1,0:T(8,128)S(1)}) custom-call(s32[6]{0:T(128)S(1)} %pad_add_fusion.ids, bf16[24,2048]{1,0:T(8,128)(2,1)S(1)} %copy-done, bf16[24,2048]{1,0:T(8,128)(2,1)S(1)} %get-tuple-element.31.part_a, bf16[24,2048]{1,0:T(8,128)(2,1)S(1)} %collective-permute-done.part_b, ...), custom_call_target="tpu_custom_call" | custom-call | tf_op jit(solution)/shard_map/pallas_call | solution.py:61
  9.8 5.0 %collective-permute-start.3 = (bf16[24,1152]{1,0:T(8,128)(2,1)S(1)}, bf16[24,1152]{1,0:T(8,128)(2,1)S(1)}, u32[]{:S(2)}, u32[]{:S(2)}) collective-permute-start(bf16[24,1152]{1,0:T(8,128)(2,1)S(1)} %get-tuple-element.32.anchor), channel_id=1, source_target_pairs={{0,24},{2,26},{4,28},{6,30},{8,16},{10,18},{12,20},{14,22},{16,8},... | collective-permute-start | bytes 165896 | tf_op jit(solution)/shard_map/ppermute | solution.py:489
  14.8 0.0 collective-permute-start.2
  14.8 0.6 collective-permute-start.1
  15.5 3.5 %collective-permute-done.1 = bf16[24,1152]{1,0:T(8,128)(2,1)S(1)} collective-permute-done((bf16[24,1152]{1,0:T(8,128)(2,1)S(1)}, bf16[24,1152]{1,0:T(8,128)(2,1)S(1)}, u32[]{:S(2)}, u32[]{:S(2)}) %collective-permute-start.1) | collective-permute-done | bytes 55328 | tf_op jit(solution)/shard_map/ppermute | solution.py:489
  19.0 1.0 %collective-permute-done.2 = bf16[24,1152]{1,0:T(8,128)(2,1)S(1)} collective-permute-done((bf16[24,1152]{1,0:T(8,128)(2,1)S(1)}, bf16[24,1152]{1,0:T(8,128)(2,1)S(1)}, u32[]{:S(2)}, u32[]{:S(2)}) %collective-permute-start.2) | collective-permute-done | bytes 55328 | tf_op jit(solution)/shard_map/ppermute | solution.py:489
  20.0 0.0 collective-permute-done.3
  20.0 2.8 %shard_map.259 = (bf16[4,64,24]{2,1,0:T(8,128)(2,1)S(1)}, bf16[512,1024]{1,0:T(8,128)(2,1)S(1)}, bf16[512,1024]{1,0:T(8,128)(2,1)S(1)}, bf16[1024,1024]{1,0:T(8,128)(2,1)S(1)}) custom-call(s32[6]{0:T(128)S(1)} %pad_add_fusion.ids, bf16[96,1152]{1,0:T(8,128)(2,1)S(1)} %constant_dynamic-update-slice_fusion.refs_0_.column, bf16[512,2048]{1,0:T(8,128)(2,1)} %down_in.1, ...), custom_call_target="tpu_custom_call" | custom-call | tf_op jit(solution)/shard_map/pallas_call | solution.py:61
  22.8 0.1 collective-permute-start.8
  22.9 2.5 %collective-permute-start.4 = (bf16[96,1152]{1,0:T(8,128)(2,1)S(1)}, bf16[96,1152]{1,0:T(8,128)(2,1)S(1)}, u32[]{:S(2)}, u32[]{:S(2)}) collective-permute-start(bf16[96,1152]{1,0:T(8,128)(2,1)S(1)} %constant_dynamic-update-slice_fusion.refs_0_.column), channel_id=1, source_target_pairs={{0,6},{2,4},{4,2},{6,0},{8,14},{10,12},{12,10},{14,8},{16,22},{18,... | collective-permute-start | bytes 663560 | tf_op jit(solution)/shard_map/ppermute | solution.py:489
  25.4 0.5 collective-permute-start.10
  25.9 0.5 collective-permute-start.9
  26.4 0.0 collective-permute-start.5
  26.4 5.8 %collective-permute-done.4.refs_1_ = bf16[96,1152]{1,0:T(8,128)(2,1)S(1)} collective-permute-done((bf16[96,1152]{1,0:T(8,128)(2,1)S(1)}, bf16[96,1152]{1,0:T(8,128)(2,1)S(1)}, u32[]{:S(2)}, u32[]{:S(2)}) %collective-permute-start.4) | collective-permute-done | bytes 221216 | tf_op jit(solution)/shard_map/ppermute | solution.py:489
  32.2 0.0 collective-permute-start.6
  32.2 4.3 %collective-permute-done.10.refs_1_ = bf16[96,1152]{1,0:T(8,128)(2,1)S(1)} collective-permute-done((bf16[96,1152]{1,0:T(8,128)(2,1)S(1)}, bf16[96,1152]{1,0:T(8,128)(2,1)S(1)}, u32[]{:S(2)}, u32[]{:S(2)}) %collective-permute-start.10) | collective-permute-done | bytes 221216 | tf_op jit(solution)/shard_map/ppermute | solution.py:489
  36.4 0.0 collective-permute-start.12
  36.4 0.0 collective-permute-done.9.refs_0_
  36.4 0.5 collective-permute-start.11
  36.9 3.5 %shard_map.257 = (bf16[2048,512]{1,0:T(8,128)(2,1)S(1)}, bf16[2048,512]{1,0:T(8,128)(2,1)S(1)}, bf16[2048,512]{1,0:T(8,128)(2,1)S(1)}, bf16[2048,512]{1,0:T(8,128)(2,1)S(1)}) custom-call(bf16[24,1152]{1,0:T(8,128)(2,1)S(1)} %get-tuple-element.32.anchor, bf16[2048,512]{1,0:T(8,128)(2,1)} %refs_0_.1, bf16[2048,512]{1,0:T(8,128)(2,1)} %refs_1_.1, ...), custom_call_target="tpu_custom_call" | custom-call | tf_op jit(solution)/shard_map/pallas_call | solution.py:61
  40.5 0.0 collective-permute-done.5.refs_2_
  40.5 0.0 collective-permute-done.6.refs_3_
  40.5 2.4 %shard_map.258 = (bf16[248,512]{1,0:T(8,128)(2,1)S(1)}, f32[48,128]{1,0:T(8,128)S(1)}) custom-call(s32[6]{0:T(128)S(1)} %pad_add_fusion.ids, bf16[96,1152]{1,0:T(8,128)(2,1)S(1)} %constant_dynamic-update-slice_fusion.refs_0_.column, bf16[96,1152]{1,0:T(8,128)(2,1)S(1)} %collective-permute-done.4.refs_1_, ...), custom_call_target="tpu_custom_call" | custom-call | tf_op jit(solution)/shard_map/pallas_call | solution.py:61
  42.9 0.1 collective-permute-start.7
  43.0 0.0 collective-permute-done.12.refs_3_
  43.0 0.0 collective-permute-done.11.refs_2_
  43.0 2.5 %shard_map.261 = (bf16[248,512]{1,0:T(8,128)(2,1)S(1)}, f32[48,128]{1,0:T(8,128)S(1)}) custom-call(s32[6]{0:T(128)S(1)} %pad_add_fusion.ids, bf16[96,1152]{1,0:T(8,128)(2,1)S(1)} %collective-permute-done.9.refs_0_, bf16[96,1152]{1,0:T(8,128)(2,1)S(1)} %collective-permute-done.10.refs_1_, bf16[96,1152]{1,0:T(8,128)(2,1)S(1)} %collective-permute-done.11.refs_2_, ...), custom_call_target="tpu_custom_call" | custom-call | tf_op jit(solution)/shard_map/pallas_call | solution.py:61
  45.5 0.5 collective-permute-start.13
  46.0 0.0 collective-permute-done.7.other
  46.0 0.0 collective-permute-done.8.down_got
  46.0 0.9 %shard_map.260 = (bf16[128,1024]{1,0:T(8,128)(2,1)S(1)}, bf16[128,1024]{1,0:T(8,128)(2,1)S(1)}) custom-call(bf16[248,512]{1,0:T(8,128)(2,1)S(1)} %get-tuple-element.37.own, bf16[248,512]{1,0:T(8,128)(2,1)S(1)} %collective-permute-done.7.other, bf16[512,1024]{1,0:T(8,128)(2,1)S(1)} %get-tuple-element.38.down_own, ...), custom_call_target="tpu_custom_call" | custom-call | tf_op jit(solution)/shard_map/pallas_call | solution.py:61
  47.0 1.9 %collective-permute-start.16 = (bf16[128,1024]{1,0:T(8,128)(2,1)S(1)}, bf16[128,1024]{1,0:T(8,128)(2,1)S(1)}, u32[]{:S(2)}, u32[]{:S(2)}) collective-permute-start(bf16[128,1024]{1,0:T(8,128)(2,1)S(1)} %get-tuple-element.47), channel_id=1, source_target_pairs={{0,6},{2,4},{4,2},{6,0},{8,14},{10,12},{12,10},{14,8},{16,22},{18,... | collective-permute-start | bytes 786440 | tf_op jit(solution)/shard_map/ppermute | solution.py:489
  48.9 0.0 collective-permute-done.13.other
  48.9 0.9 %shard_map.262 = (bf16[128,1024]{1,0:T(8,128)(2,1)S(1)}, bf16[128,1024]{1,0:T(8,128)(2,1)S(1)}) custom-call(bf16[248,512]{1,0:T(8,128)(2,1)S(1)} %get-tuple-element.43.own, bf16[248,512]{1,0:T(8,128)(2,1)S(1)} %collective-permute-done.13.other, bf16[512,1024]{1,0:T(8,128)(2,1)S(1)} %get-tuple-element.38.down_own, ...), custom_call_target="tpu_custom_call" | custom-call | tf_op jit(solution)/shard_map/pallas_call | solution.py:61
  49.8 0.6 collective-permute-start.14
  50.4 1.1 %collective-permute-start.15 = (bf16[128,1024]{1,0:T(8,128)(2,1)S(1)}, bf16[128,1024]{1,0:T(8,128)(2,1)S(1)}, u32[]{:S(2)}, u32[]{:S(2)}) collective-permute-start(bf16[128,1024]{1,0:T(8,128)(2,1)S(1)} %get-tuple-element.46), channel_id=1, source_target_pairs={{0,4},{2,6},{4,0},{6,2},{8,12},{10,14},{12,8},{14,10},{16,20},{18,... | collective-permute-start | bytes 786440 | tf_op jit(solution)/shard_map/ppermute | solution.py:489
  51.5 0.6 copy.61
  52.1 0.6 copy.62
  52.7 0.7 copy.56
  53.4 3.8 %collective-permute-done.16.refs_3_ = bf16[128,1024]{1,0:T(8,128)(2,1)S(1)} collective-permute-done((bf16[128,1024]{1,0:T(8,128)(2,1)S(1)}, bf16[128,1024]{1,0:T(8,128)(2,1)S(1)}, u32[]{:S(2)}, u32[]{:S(2)}) %collective-permute-start.16) | collective-permute-done | bytes 262176 | tf_op jit(solution)/shard_map/ppermute | solution.py:489
  57.1 4.6 %collective-permute-done.14.refs_1_ = bf16[128,1024]{1,0:T(8,128)(2,1)S(1)} collective-permute-done((bf16[128,1024]{1,0:T(8,128)(2,1)S(1)}, bf16[128,1024]{1,0:T(8,128)(2,1)S(1)}, u32[]{:S(2)}, u32[]{:S(2)}) %collective-permute-start.14) | collective-permute-done | bytes 262176 | tf_op jit(solution)/shard_map/ppermute | solution.py:489
  61.7 0.0 collective-permute-done.15.refs_2_
  61.8 0.3 shard_map.263
  62.0 1.3 %collective-permute-start.17 = (bf16[40,1024]{1,0:T(8,128)(2,1)S(1)}, bf16[40,1024]{1,0:T(8,128)(2,1)S(1)}, u32[]{:S(2)}, u32[]{:S(2)}) collective-permute-start(bf16[40,1024]{1,0:T(8,128)(2,1)S(1)} %get-tuple-element.50), channel_id=1, source_target_pairs={{0,8},{2,10},{4,12},{6,14},{8,0},{10,2},{12,4},{14,6},{16,24},{18,... | collective-permute-start | bytes 245768 | tf_op jit(solution)/shard_map/ppermute | solution.py:489
  63.3 1.8 %collective-permute-start.18 = (bf16[40,1024]{1,0:T(8,128)(2,1)S(1)}, bf16[40,1024]{1,0:T(8,128)(2,1)S(1)}, u32[]{:S(2)}, u32[]{:S(2)}) collective-permute-start(bf16[40,1024]{1,0:T(8,128)(2,1)S(1)} %get-tuple-element.51), channel_id=1, source_target_pairs={{0,16},{2,18},{4,20},{6,22},{8,24},{10,26},{12,28},{14,30},{16,0},... | collective-permute-start | bytes 245768 | tf_op jit(solution)/shard_map/ppermute | solution.py:489
  65.1 1.4 %collective-permute-start.19 = (bf16[40,1024]{1,0:T(8,128)(2,1)S(1)}, bf16[40,1024]{1,0:T(8,128)(2,1)S(1)}, u32[]{:S(2)}, u32[]{:S(2)}) collective-permute-start(bf16[40,1024]{1,0:T(8,128)(2,1)S(1)} %get-tuple-element.52), channel_id=1, source_target_pairs={{0,24},{2,26},{4,28},{6,30},{8,16},{10,18},{12,20},{14,22},{16,8},... | collective-permute-start | bytes 245768 | tf_op jit(solution)/shard_map/ppermute | solution.py:489
  66.5 0.0 collective-permute-done.17.refs_2_
  66.6 6.1 %collective-permute-done.18.refs_3_ = bf16[40,1024]{1,0:T(8,128)(2,1)S(1)} collective-permute-done((bf16[40,1024]{1,0:T(8,128)(2,1)S(1)}, bf16[40,1024]{1,0:T(8,128)(2,1)S(1)}, u32[]{:S(2)}, u32[]{:S(2)}) %collective-permute-start.18) | collective-permute-done | bytes 81952 | tf_op jit(solution)/shard_map/ppermute | solution.py:489
  72.6 0.0 collective-permute-done.19.refs_4_
  72.6 0.8 %shard_map.264 = bf16[24,1024]{1,0:T(8,128)(2,1)S(1)} custom-call(s32[4]{0:T(128)S(1)} %iota_xor_fusion.refs_0_, bf16[40,1024]{1,0:T(8,128)(2,1)S(1)} %get-tuple-element.49.refs_1_, bf16[40,1024]{1,0:T(8,128)(2,1)S(1)} %collective-permute-done.17.refs_2_, bf16[40,1024]{1,0:T(8,128)(2,1)S(1)} %collective-permute-done.18.refs_3_, ...), custom_call_target="tpu_custom_call" | custom-call | tf_op jit(solution)/shard_map/pallas_call | solution.py:61
  73.4 0.6 copy.60
  (18 shorter events, 0.1 us)
Async XLA Ops:
  0.7 7.3 %copy-start.3 = (s32[24,2]{0,1:T(2,128)S(1)}, s32[24,2]{0,1:T(2,128)}, u32[]{:S(2)}) copy-start(s32[24,2]{0,1:T(2,128)} %param.43) | copy-start | bytes 580
  0.7 7.4 %copy-start.4 = (f32[24,2]{0,1:T(2,128)S(1)}, f32[24,2]{0,1:T(2,128)}, u32[]{:S(2)}) copy-start(f32[24,2]{0,1:T(2,128)} %param.44) | copy-start | bytes 580
  0.7 8.2 %copy-start = (bf16[24,2048]{1,0:T(8,128)(2,1)S(1)}, bf16[24,2048]{1,0:T(8,128)(2,1)}, u32[]{:S(2)}) copy-start(bf16[24,2048]{1,0:T(8,128)(2,1)} %tokens.1) | copy-start | bytes 294916
  0.8 8.2 %copy-start.1 = (bf16[2048]{0:T(1024)(128)(2,1)S(1)}, bf16[2048]{0:T(1024)(128)(2,1)}, u32[]{:S(2)}) copy-start(bf16[2048]{0:T(1024)(128)(2,1)} %gain.1) | copy-start | bytes 12292
  0.8 8.2 %copy-start.2 = (bf16[2048]{0:T(1024)(128)(2,1)S(1)}, bf16[2048]{0:T(1024)(128)(2,1)}, u32[]{:S(2)}) copy-start(bf16[2048]{0:T(1024)(128)(2,1)} %branch_gate.1) | copy-start | bytes 12292
  7.5 1.5 %collective-permute-start = (bf16[24,2048]{1,0:T(8,128)(2,1)S(1)}, bf16[24,2048]{1,0:T(8,128)(2,1)S(1)}, u32[]{:S(2)}, u32[]{:S(2)}) collective-permute-start(bf16[24,2048]{1,0:T(8,128)(2,1)S(1)} %get-tuple-element.31.part_a), channel_id=1, source_target_pairs={{0,1},{1,0},{2,3},{3,2},{4,5},{5,4},{6,7},{7,6},{8,9},{9,8},{10,11... | collective-permute-start | bytes 294920 | tf_op jit(solution)/shard_map/ppermute | solution.py:486
  9.8 10.2 %collective-permute-start.3 = (bf16[24,1152]{1,0:T(8,128)(2,1)S(1)}, bf16[24,1152]{1,0:T(8,128)(2,1)S(1)}, u32[]{:S(2)}, u32[]{:S(2)}) collective-permute-start(bf16[24,1152]{1,0:T(8,128)(2,1)S(1)} %get-tuple-element.32.anchor), channel_id=1, source_target_pairs={{0,24},{2,26},{4,28},{6,30},{8,16},{10,18},{12,20},{14,22},{16,8},... | collective-permute-start | bytes 165896 | tf_op jit(solution)/shard_map/ppermute | solution.py:489
  14.8 5.2 %collective-permute-start.2 = (bf16[24,1152]{1,0:T(8,128)(2,1)S(1)}, bf16[24,1152]{1,0:T(8,128)(2,1)S(1)}, u32[]{:S(2)}, u32[]{:S(2)}) collective-permute-start(bf16[24,1152]{1,0:T(8,128)(2,1)S(1)} %get-tuple-element.32.anchor), channel_id=1, source_target_pairs={{0,16},{2,18},{4,20},{6,22},{8,24},{10,26},{12,28},{14,30},{16,0},... | collective-permute-start | bytes 165896 | tf_op jit(solution)/shard_map/ppermute | solution.py:489
  14.8 4.2 %collective-permute-start.1 = (bf16[24,1152]{1,0:T(8,128)(2,1)S(1)}, bf16[24,1152]{1,0:T(8,128)(2,1)S(1)}, u32[]{:S(2)}, u32[]{:S(2)}) collective-permute-start(bf16[24,1152]{1,0:T(8,128)(2,1)S(1)} %get-tuple-element.32.anchor), channel_id=1, source_target_pairs={{0,8},{2,10},{4,12},{6,14},{8,0},{10,2},{12,4},{14,6},{16,24},{18,... | collective-permute-start | bytes 165896 | tf_op jit(solution)/shard_map/ppermute | solution.py:489
  22.8 23.2 %collective-permute-start.8 = (bf16[1024,1024]{1,0:T(8,128)(2,1)S(1)}, bf16[1024,1024]{1,0:T(8,128)(2,1)S(1)}, u32[]{:S(2)}, u32[]{:S(2)}) collective-permute-start(bf16[1024,1024]{1,0:T(8,128)(2,1)S(1)} %get-tuple-element.40), channel_id=1, source_target_pairs={{0,1},{1,0},{2,3},{3,2},{4,5},{5,4},{6,7},{7,6},{8,9},{9,8},{10,11... | collective-permute-start | bytes 6291464 | tf_op jit(solution)/shard_map/ppermute | solution.py:486
  22.9 9.3 %collective-permute-start.4 = (bf16[96,1152]{1,0:T(8,128)(2,1)S(1)}, bf16[96,1152]{1,0:T(8,128)(2,1)S(1)}, u32[]{:S(2)}, u32[]{:S(2)}) collective-permute-start(bf16[96,1152]{1,0:T(8,128)(2,1)S(1)} %constant_dynamic-update-slice_fusion.refs_0_.column), channel_id=1, source_target_pairs={{0,6},{2,4},{4,2},{6,0},{8,14},{10,12},{12,10},{14,8},{16,22},{18,... | collective-permute-start | bytes 663560 | tf_op jit(solution)/shard_map/ppermute | solution.py:489
  25.4 11.1 %collective-permute-start.10 = (bf16[96,1152]{1,0:T(8,128)(2,1)S(1)}, bf16[96,1152]{1,0:T(8,128)(2,1)S(1)}, u32[]{:S(2)}, u32[]{:S(2)}) collective-permute-start(bf16[96,1152]{1,0:T(8,128)(2,1)S(1)} %constant_dynamic-update-slice_fusion.refs_0_.column), channel_id=1, source_target_pairs={{0,2},{2,0},{4,6},{6,4},{8,10},{10,8},{12,14},{14,12},{16,18},{18,... | collective-permute-start | bytes 663560 | tf_op jit(solution)/shard_map/ppermute | solution.py:489
  25.9 10.5 %collective-permute-start.9 = (bf16[96,1152]{1,0:T(8,128)(2,1)S(1)}, bf16[96,1152]{1,0:T(8,128)(2,1)S(1)}, u32[]{:S(2)}, u32[]{:S(2)}) collective-permute-start(bf16[96,1152]{1,0:T(8,128)(2,1)S(1)} %constant_dynamic-update-slice_fusion.refs_0_.column), channel_id=1, source_target_pairs={{0,4},{2,6},{4,0},{6,2},{8,12},{10,14},{12,8},{14,10},{16,20},{18,... | collective-permute-start | bytes 663560 | tf_op jit(solution)/shard_map/ppermute | solution.py:489
  26.4 14.0 %collective-permute-start.5 = (bf16[96,1152]{1,0:T(8,128)(2,1)S(1)}, bf16[96,1152]{1,0:T(8,128)(2,1)S(1)}, u32[]{:S(2)}, u32[]{:S(2)}) collective-permute-start(bf16[96,1152]{1,0:T(8,128)(2,1)S(1)} %constant_dynamic-update-slice_fusion.refs_0_.column), channel_id=1, source_target_pairs={{0,1},{1,0},{2,3},{3,2},{4,5},{5,4},{6,7},{7,6},{8,9},{9,8},{10,11... | collective-permute-start | bytes 663560 | tf_op jit(solution)/shard_map/ppermute | solution.py:486
  32.2 8.3 %collective-permute-start.6 = (bf16[96,1152]{1,0:T(8,128)(2,1)S(1)}, bf16[96,1152]{1,0:T(8,128)(2,1)S(1)}, u32[]{:S(2)}, u32[]{:S(2)}) collective-permute-start(bf16[96,1152]{1,0:T(8,128)(2,1)S(1)} %collective-permute-done.4.refs_1_), channel_id=1, source_target_pairs={{0,1},{1,0},{2,3},{3,2},{4,5},{5,4},{6,7},{7,6},{8,9},{9,8},{10,11... | collective-permute-start | bytes 663560 | tf_op jit(solution)/shard_map/ppermute | solution.py:486
  36.4 6.6 %collective-permute-start.12 = (bf16[96,1152]{1,0:T(8,128)(2,1)S(1)}, bf16[96,1152]{1,0:T(8,128)(2,1)S(1)}, u32[]{:S(2)}, u32[]{:S(2)}) collective-permute-start(bf16[96,1152]{1,0:T(8,128)(2,1)S(1)} %collective-permute-done.10.refs_1_), channel_id=1, source_target_pairs={{0,1},{1,0},{2,3},{3,2},{4,5},{5,4},{6,7},{7,6},{8,9},{9,8},{10,11... | collective-permute-start | bytes 663560 | tf_op jit(solution)/shard_map/ppermute | solution.py:486
  36.4 6.6 %collective-permute-start.11 = (bf16[96,1152]{1,0:T(8,128)(2,1)S(1)}, bf16[96,1152]{1,0:T(8,128)(2,1)S(1)}, u32[]{:S(2)}, u32[]{:S(2)}) collective-permute-start(bf16[96,1152]{1,0:T(8,128)(2,1)S(1)} %collective-permute-done.9.refs_0_), channel_id=1, source_target_pairs={{0,1},{1,0},{2,3},{3,2},{4,5},{5,4},{6,7},{7,6},{8,9},{9,8},{10,11... | collective-permute-start | bytes 663560 | tf_op jit(solution)/shard_map/ppermute | solution.py:486
  42.9 3.1 %collective-permute-start.7 = (bf16[248,512]{1,0:T(8,128)(2,1)S(1)}, bf16[248,512]{1,0:T(8,128)(2,1)S(1)}, u32[]{:S(2)}, u32[]{:S(2)}) collective-permute-start(bf16[248,512]{1,0:T(8,128)(2,1)S(1)} %get-tuple-element.37.own), channel_id=1, source_target_pairs={{0,1},{1,0},{2,3},{3,2},{4,5},{5,4},{6,7},{7,6},{8,9},{9,8},{10,11... | collective-permute-start | bytes 761864 | tf_op jit(solution)/shard_map/ppermute | solution.py:486
  45.5 3.4 %collective-permute-start.13 = (bf16[248,512]{1,0:T(8,128)(2,1)S(1)}, bf16[248,512]{1,0:T(8,128)(2,1)S(1)}, u32[]{:S(2)}, u32[]{:S(2)}) collective-permute-start(bf16[248,512]{1,0:T(8,128)(2,1)S(1)} %get-tuple-element.43.own), channel_id=1, source_target_pairs={{0,1},{1,0},{2,3},{3,2},{4,5},{5,4},{6,7},{7,6},{8,9},{9,8},{10,11... | collective-permute-start | bytes 761864 | tf_op jit(solution)/shard_map/ppermute | solution.py:486
  47.0 10.2 %collective-permute-start.16 = (bf16[128,1024]{1,0:T(8,128)(2,1)S(1)}, bf16[128,1024]{1,0:T(8,128)(2,1)S(1)}, u32[]{:S(2)}, u32[]{:S(2)}) collective-permute-start(bf16[128,1024]{1,0:T(8,128)(2,1)S(1)} %get-tuple-element.47), channel_id=1, source_target_pairs={{0,6},{2,4},{4,2},{6,0},{8,14},{10,12},{12,10},{14,8},{16,22},{18,... | collective-permute-start | bytes 786440 | tf_op jit(solution)/shard_map/ppermute | solution.py:489
  49.8 11.9 %collective-permute-start.14 = (bf16[128,1024]{1,0:T(8,128)(2,1)S(1)}, bf16[128,1024]{1,0:T(8,128)(2,1)S(1)}, u32[]{:S(2)}, u32[]{:S(2)}) collective-permute-start(bf16[128,1024]{1,0:T(8,128)(2,1)S(1)} %get-tuple-element.45), channel_id=1, source_target_pairs={{0,2},{2,0},{4,6},{6,4},{8,10},{10,8},{12,14},{14,12},{16,18},{18,... | collective-permute-start | bytes 786440 | tf_op jit(solution)/shard_map/ppermute | solution.py:489
  50.4 11.4 %collective-permute-start.15 = (bf16[128,1024]{1,0:T(8,128)(2,1)S(1)}, bf16[128,1024]{1,0:T(8,128)(2,1)S(1)}, u32[]{:S(2)}, u32[]{:S(2)}) collective-permute-start(bf16[128,1024]{1,0:T(8,128)(2,1)S(1)} %get-tuple-element.46), channel_id=1, source_target_pairs={{0,4},{2,6},{4,0},{6,2},{8,12},{10,14},{12,8},{14,10},{16,20},{18,... | collective-permute-start | bytes 786440 | tf_op jit(solution)/shard_map/ppermute | solution.py:489
  62.0 4.5 %collective-permute-start.17 = (bf16[40,1024]{1,0:T(8,128)(2,1)S(1)}, bf16[40,1024]{1,0:T(8,128)(2,1)S(1)}, u32[]{:S(2)}, u32[]{:S(2)}) collective-permute-start(bf16[40,1024]{1,0:T(8,128)(2,1)S(1)} %get-tuple-element.50), channel_id=1, source_target_pairs={{0,8},{2,10},{4,12},{6,14},{8,0},{10,2},{12,4},{14,6},{16,24},{18,... | collective-permute-start | bytes 245768 | tf_op jit(solution)/shard_map/ppermute | solution.py:489
  63.3 9.3 %collective-permute-start.18 = (bf16[40,1024]{1,0:T(8,128)(2,1)S(1)}, bf16[40,1024]{1,0:T(8,128)(2,1)S(1)}, u32[]{:S(2)}, u32[]{:S(2)}) collective-permute-start(bf16[40,1024]{1,0:T(8,128)(2,1)S(1)} %get-tuple-element.51), channel_id=1, source_target_pairs={{0,16},{2,18},{4,20},{6,22},{8,24},{10,26},{12,28},{14,30},{16,0},... | collective-permute-start | bytes 245768 | tf_op jit(solution)/shard_map/ppermute | solution.py:489
  65.1 7.5 %collective-permute-start.19 = (bf16[40,1024]{1,0:T(8,128)(2,1)S(1)}, bf16[40,1024]{1,0:T(8,128)(2,1)S(1)}, u32[]{:S(2)}, u32[]{:S(2)}) collective-permute-start(bf16[40,1024]{1,0:T(8,128)(2,1)S(1)} %get-tuple-element.52), channel_id=1, source_target_pairs={{0,24},{2,26},{4,28},{6,30},{8,16},{10,18},{12,20},{14,22},{16,8},... | collective-permute-start | bytes 245768 | tf_op jit(solution)/shard_map/ppermute | solution.py:489

commit v2 on v1

--- a/solution.py
+++ b/solution.py
@@ -45,7 +45,7 @@
 SMEM = pl.BlockSpec(memory_space=pltpu.SMEM)
 
 
-def call(kernel, outs, operands, hbm=(), scratch=(), limit=20):
+def call(kernel, outs, operands, hbm=(), scratch=(), limit=20, kept=True):
     specs = []
     held = []
     for index, op in enumerate(operands):
@@ -62,7 +62,7 @@
         kernel,
         in_specs=specs,
         out_specs=[VMEM] * len(outs),
-        out_shape=[pltpu.VMEM(shape, dtype) for shape, dtype in outs],
+        out_shape=[(pltpu.VMEM if kept else jax.ShapeDtypeStruct)(shape, dtype) for shape, dtype in outs],
         scratch_shapes=list(scratch),
         compiler_params=pltpu.CompilerParams(vmem_limit_bytes=limit * 1024 * 1024),
     )(*held)
@@ -111,34 +111,38 @@
     resid[...] = jnp.where(first, total[:, :half], total[:, half:]).astype(BF16)
 
 
-def fetch_kernel(anchor, *refs):
-    count = (len(refs) - 1) // 2
-    copies = [
-        pltpu.make_async_copy(refs[i], refs[count + i], refs[-1].at[i]) for i in range(count)
+def fetch_kernel(
+    ids, anchor, gate_in, up_in, expert_gate_in, expert_up_in, down_in, expert_in,
+    down_sent, gate_w, up_w, expert_gate, expert_up, sems,
+):
+    hidden, half = down_in.shape[0], down_sent.shape[1]
+    other = expert_in.shape[0]
+    theirs = pl.ds(pl.multiple_of((1 - ids[0]) * half, half), half)
+    pairs = [
+        (down_in.at[:, theirs], down_sent.at[pl.ds(0, hidden)]),
+        (expert_in.at[:, theirs], down_sent.at[pl.ds(hidden, other)]),
+        (gate_in, gate_w), (up_in, up_w), (expert_gate_in, expert_gate),
+        (expert_up_in, expert_up),
     ]
+    copies = [pltpu.make_async_copy(a, b, sems.at[i]) for i, (a, b) in enumerate(pairs)]
     for copy in copies:
         copy.start()
     for copy in copies:
         copy.wait()
 
 
-def load_kernel(
-    ids, column, down_in, expert_in, combine, down_own, expert_own, down_sent, sems,
-    *, seq, capacity, top_k,
-):
-    hidden, half = down_own.shape
-    other = expert_own.shape[0]
+def load_kernel(ids, column, down_in, expert_in, down_own, expert_own, sems):
+    half = down_own.shape[1]
     mine = pl.ds(pl.multiple_of(ids[0] * half, half), half)
-    theirs = pl.ds(pl.multiple_of((1 - ids[0]) * half, half), half)
-    pairs = [
-        (down_in.at[:, theirs], down_sent.at[pl.ds(0, hidden)]),
-        (expert_in.at[:, theirs], down_sent.at[pl.ds(hidden, other)]),
-        (down_in.at[:, mine], down_own),
-        (expert_in.at[:, mine], expert_own),
-    ]
+    pairs = [(down_in.at[:, mine], down_own), (expert_in.at[:, mine], expert_own)]
     copies = [pltpu.make_async_copy(a, b, sems.at[i]) for i, (a, b) in enumerate(pairs)]
     for copy in copies:
         copy.start()
+    for copy in copies:
+        copy.wait()
+
+
+def table_kernel(ids, column, combine, *, seq, capacity, top_k):
     plane = combine.shape[0]
     planes = combine.shape[2] // capacity
     pair_rows = combine.shape[1] // planes
@@ -160,31 +164,25 @@
                 info[:, k : k + 1] + near_key == lane_key + ids[2 + j].astype(F32)
             ).astype(F32)
         combine[j] = dot(joined, match.astype(BF16)).astype(BF16)
-    for copy in copies:
-        copy.wait()
 
 
 def hidden_kernel(ids, *refs, seq, capacity, top_k):
-    plane = (len(refs) - 9) // 2
+    plane = (len(refs) - 8) // 2
     owns, others = refs[:plane], refs[plane : 2 * plane]
-    gate_w, up_w, expert_gate, expert_up, out, slot_weight, lefts, rights, notes = refs[2 * plane :]
-    count, half = lefts.shape
+    gate_w, up_w, expert_gate, expert_up, out, slot_weight, tokens, notes = refs[2 * plane :]
+    count = tokens.shape[0]
+    half = tokens.shape[1] // 2
     slots = slot_weight.shape[0]
     group = count // plane
+    own_part = pl.ds(pl.multiple_of(ids[0] * half, half), half)
+    other_part = pl.ds(pl.multiple_of((1 - ids[0]) * half, half), half)
     for j in range(plane):
         rows = pl.ds(j * group, group)
-        lefts[rows, :] = owns[j][:, :half]
-        rights[rows, :] = others[j][:, :half]
+        tokens[rows, own_part] = owns[j][:, :half]
+        tokens[rows, other_part] = others[j][:, :half]
         notes[rows, :] = owns[j][:, half:].astype(F32)
-    own_rows = pl.ds(pl.multiple_of(ids[0] * half, half), half)
-    other_rows = pl.ds(pl.multiple_of((1 - ids[0]) * half, half), half)
-    left = lefts[...]
-    right = rights[...]
-
-    def project(rows_own, rows_other, weight):
-        return dot(rows_own, weight[own_rows, :]) + dot(rows_other, weight[other_rows, :])
-
-    hidden = silu(project(left, right, gate_w)) * project(left, right, up_w)
+    all_rows = tokens[...]
+    hidden = silu(dot(all_rows, gate_w[...])) * dot(all_rows, up_w[...])
     out[0:count, 0 : gate_w.shape[1]] = hidden.astype(BF16)
     squares = jnp.sum(hidden * hidden, axis=1, keepdims=True)
     extra = out.shape[0] - count - slots
@@ -213,11 +211,8 @@
         jnp.sum(weight, axis=1, keepdims=True), slot_weight.shape
     )
     pick = pick.astype(BF16)
-    rows_own = dot(pick, left).astype(BF16)
-    rows_other = dot(pick, right).astype(BF16)
-    active = silu(project(rows_own, rows_other, expert_gate)) * project(
-        rows_own, rows_other, expert_up
-    )
+    picked = dot(pick, all_rows).astype(BF16)
+    active = silu(dot(picked, expert_gate[...])) * dot(picked, expert_up[...])
     out[count : count + slots, 0 : expert_gate.shape[1]] = active.astype(BF16)
 
 
@@ -506,40 +501,41 @@
         [((seq, half + LANES), BF16), ((seq, half), BF16), ((seq, LANES), F32)],
         [ids, tokens, partial, swap(partial), post_gain, branch_gate, notes],
     )
-    near = []
-    for k in range(1, planes):
-        near.append(exchange(payload, k * plane))
+    near = [None] * planes
+    for k in reversed(range(1, planes)):
+        near[k] = exchange(payload, k * plane)
     wide = [dense_gate_w, dense_up_w, expert_gate_w[0], expert_up_w[0]]
-    gate_w, up_w, expert_gate, expert_up = call(
+    down_sent, gate_w, up_w, expert_gate, expert_up = call(
         fetch_kernel,
-        [(value.shape, BF16) for value in wide],
-        [payload, *wide],
-        hbm=range(1, 5),
-        scratch=[pltpu.SemaphoreType.DMA((4,))],
-    )
-    column = jnp.concatenate([payload] + near, axis=0)
+        [((ff_local + expert_local, half), BF16)] + [(value.shape, BF16) for value in wide],
+        [ids, payload, *wide, dense_down_w, expert_down_w[0]],
+        hbm=range(2, 8),
+        scratch=[pltpu.SemaphoreType.DMA((6,))],
+    )
+    column = jnp.concatenate([payload] + near[1:], axis=0)
     owns = [column] + [None] * (plane - 1)
     for j in reversed(range(1, plane)):
         owns[j] = exchange(column, j)
-    combine, down_own, expert_own, down_sent = call(
-        functools.partial(load_kernel, seq=seq, capacity=capacity, top_k=top_k),
-        [
-            ((plane, planes * pair_rows, planes * capacity), BF16),
-            ((ff_local, half), BF16),
-            ((expert_local, half), BF16),
-            ((ff_local + expert_local, half), BF16),
-        ],
+    down_own, expert_own = call(
+        load_kernel,
+        [((ff_local, half), BF16), ((expert_local, half), BF16)],
         [ids, column, dense_down_w, expert_down_w[0]],
         hbm=range(2, 4),
-        scratch=[pltpu.SemaphoreType.DMA((4,))],
+        scratch=[pltpu.SemaphoreType.DMA((2,))],
+    )
+    (combine,) = call(
+        functools.partial(table_kernel, seq=seq, capacity=capacity, top_k=top_k),
+        [((plane, planes * pair_rows, planes * capacity), BF16)],
+        [ids, column],
     )
     down_got = swap(down_sent)
     others = []
     for j in range(plane):
         others.append(swap(owns[j]))
     arrived = [None] * plane
-    order = [0] + list(reversed(range(1, plane)))
-    for members in (order[: plane // 2], order[plane // 2 :]):
+    order = list(reversed(range(1, plane)))
+    early, late = order[: plane // 2 - 1], order[plane // 2 - 1 :]
+    for members in ([0] + early, late):
         size = len(members)
         rows, routes = size * planes * seq, size * planes * capacity
         extra = 8 * ((2 * size + 7) // 8)
@@ -551,8 +547,7 @@
                 gate_w, up_w, expert_gate, expert_up,
             ],
             scratch=[
-                pltpu.VMEM((rows, half), BF16), pltpu.VMEM((rows, half), BF16),
-                pltpu.VMEM((rows, LANES), F32),
+                pltpu.VMEM((rows, width), BF16), pltpu.VMEM((rows, LANES), F32),
             ],
         )
         hidden_other = swap(hidden)
@@ -568,13 +563,16 @@
         [((seq + pair_rows, half), BF16)] * planes,
         [*arrived, combine],
     )
-    final = [lasts[0]] + [exchange(lasts[k], k * plane) for k in range(1, planes)]
+    final = [lasts[0]] + [None] * (planes - 1)
+    for k in reversed(range(1, planes)):
+        final[k] = exchange(lasts[k], k * plane)
     (mixed_out,) = call(
         functools.partial(
             final_kernel, ff_total=ff_total, route_base=capacity * plane, top_k=top_k
         ),
         [((seq, half), BF16)],
         [z_peers, *final, resid, branch, notes],
+        kept=True,
     )
     return (mixed_out, fresh_key, fresh_value, current)
 

time: 74.2 us -> 73.8 us (level)
  waiting for transfers between devices: 29.2 us -> 27.4 us
  Pallas kernels: 21.6 us -> 22.9 us
    ppermute x12, waiting for transfers between devices: 29 us -> 27.3 us  [exchange(): return lax.ppermute(values, 'ep', [(i, i ^ mask) for i in range(ep_count)])]
    pallas_call x10 -> x11, Pallas kernels: 21.6 us -> 22.9 us  [call(): pl.pallas_call(kernel, in_specs=specs, out_specs=[VMEM] * len(outs), out_...]
  transfers between devices with their start and end apart: 20 -> 20, of which waited for: 8 -> 10; matrix products, arithmetic and copies ran while one was open for 4% -> 4% of each run, Pallas kernels for 14% -> 13%
where the time goes in v2:
time: 73.8 us; the launch traced here: 73.7 us
  waiting for transfers between devices  27.4 us (37%)
  Pallas kernels  22.9 us (31%)
  starting transfers between devices  19.1 us (26%)
  local copies, waits for them, and re-layouts  3.09 us (4%)
  between operations  0.82 us (1%)
    ppermute x12, waiting for transfers between devices, exchange(): return lax.ppermute(values, 'ep', [(i, i ^ mask) for i in range(ep_count)])  27.3 us
    pallas_call x11, Pallas kernels, call(): pl.pallas_call(kernel, in_specs=specs, out_specs=[VMEM] * len(outs), out_...  22.9 us
    ppermute x12, starting transfers between devices, exchange(): return lax.ppermute(values, 'ep', [(i, i ^ mask) for i in range(ep_count)])  16.9 us
    unnamed x18, local copies, waits for them, and re-layouts  2.6 us
    ppermute x8, starting transfers between devices, swap(): return lax.ppermute(values, 'tp', [(i, 1 - i) for i in range(tp_count)])  2.16 us
  transfers between devices with their start and end apart: 20, of which 10 were waited for; matrix products, arithmetic and copies ran while one was open for 4% of the time, Pallas kernels for 13%

profile of v2, /device:TPU:0, one launch (start us, length us, event | category | flops | bytes accessed | tf_op | source)
XLA Modules:
  0.0 73.7 jit_solution(18235389055195006640)
XLA Ops:
  0.7 0.1 pad_add_fusion.ids
  0.8 0.0 copy-start.2
  0.8 6.7 %shard_map.255 = (bf16[24,2048]{1,0:T(8,128)(2,1)S(1)}, bf16[24,64]{1,0:T(8,128)(2,1)S(1)}, bf16[24,64]{1,0:T(8,128)(2,1)S(1)}, f32[24,8]{1,0:T(8,128)S(1)}) custom-call(s32[6]{0:T(128)S(1)} %pad_add_fusion.ids, s32[24]{0:T(128)} %lens_in.1, bf16[24,2048]{1,0:T(8,128)(2,1)} %tokens.1, bf16[2048]{0:T(1024)(128)(2,1)} %norm_in.1, bf16[64]{0:T(256)(128)(2,1)} %query_in.1, ...), custom_call_target="tpu_custom_call" | custom-call | tf_op jit(solution)/shard_map/pallas_call | solution.py:61
  7.5 0.6 collective-permute-start
  8.1 0.1 copy.52
  8.2 0.1 copy.54
  8.3 0.1 copy.55
  8.4 0.1 eq.17
  8.5 0.1 fusion
  8.6 0.1 reduce_sum.12
  8.7 0.1 copy.53
  8.8 0.1 fusion.5.notes.refs_7_
  8.9 0.1 collective-permute-done.part_b
  9.0 0.8 %shard_map.256 = (bf16[24,1152]{1,0:T(8,128)(2,1)S(1)}, bf16[24,1024]{1,0:T(8,128)(2,1)S(1)}, f32[24,128]{1,0:T(8,128)S(1)}) custom-call(s32[6]{0:T(128)S(1)} %pad_add_fusion.ids, bf16[24,2048]{1,0:T(8,128)(2,1)S(1)} %copy-done, bf16[24,2048]{1,0:T(8,128)(2,1)S(1)} %get-tuple-element.30.part_a, bf16[24,2048]{1,0:T(8,128)(2,1)S(1)} %collective-permute-done.part_b, ...), custom_call_target="tpu_custom_call" | custom-call | tf_op jit(solution)/shard_map/pallas_call | solution.py:61
  9.8 4.7 %shard_map.257 = (bf16[1024,1024]{1,0:T(8,128)(2,1)S(1)}, bf16[2048,512]{1,0:T(8,128)(2,1)S(1)}, bf16[2048,512]{1,0:T(8,128)(2,1)S(1)}, bf16[2048,512]{1,0:T(8,128)(2,1)S(1)}, bf16[2048,512]{1,0:T(8,128)(2,1)S(1)}) custom-call(s32[6]{0:T(128)S(1)} %pad_add_fusion.ids, bf16[24,1152]{1,0:T(8,128)(2,1)S(1)} %get-tuple-element.31.anchor, ...), custom_call_target="tpu_custom_call" | custom-call | tf_op jit(solution)/shard_map/pallas_call | solution.py:61
  14.5 0.4 collective-permute-start.8
  14.9 2.7 %collective-permute-start.1 = (bf16[24,1152]{1,0:T(8,128)(2,1)S(1)}, bf16[24,1152]{1,0:T(8,128)(2,1)S(1)}, u32[]{:S(2)}, u32[]{:S(2)}) collective-permute-start(bf16[24,1152]{1,0:T(8,128)(2,1)S(1)} %get-tuple-element.31.anchor), channel_id=1, source_target_pairs={{0,8},{2,10},{4,12},{6,14},{8,0},{10,2},{12,4},{14,6},{16,24},{18,... | collective-permute-start | bytes 165896 | tf_op jit(solution)/shard_map/ppermute | solution.py:484
  17.6 2.6 %collective-permute-start.2 = (bf16[24,1152]{1,0:T(8,128)(2,1)S(1)}, bf16[24,1152]{1,0:T(8,128)(2,1)S(1)}, u32[]{:S(2)}, u32[]{:S(2)}) collective-permute-start(bf16[24,1152]{1,0:T(8,128)(2,1)S(1)} %get-tuple-element.31.anchor), channel_id=1, source_target_pairs={{0,16},{2,18},{4,20},{6,22},{8,24},{10,26},{12,28},{14,30},{16,0},... | collective-permute-start | bytes 165896 | tf_op jit(solution)/shard_map/ppermute | solution.py:484
  20.2 0.0 collective-permute-start.3
  20.2 0.0 collective-permute-done.1
  20.2 3.8 %collective-permute-done.2 = bf16[24,1152]{1,0:T(8,128)(2,1)S(1)} collective-permute-done((bf16[24,1152]{1,0:T(8,128)(2,1)S(1)}, bf16[24,1152]{1,0:T(8,128)(2,1)S(1)}, u32[]{:S(2)}, u32[]{:S(2)}) %collective-permute-start.2) | collective-permute-done | bytes 55328 | tf_op jit(solution)/shard_map/ppermute | solution.py:484
  24.0 2.2 %collective-permute-done.3 = bf16[24,1152]{1,0:T(8,128)(2,1)S(1)} collective-permute-done((bf16[24,1152]{1,0:T(8,128)(2,1)S(1)}, bf16[24,1152]{1,0:T(8,128)(2,1)S(1)}, u32[]{:S(2)}, u32[]{:S(2)}) %collective-permute-start.3) | collective-permute-done | bytes 55328 | tf_op jit(solution)/shard_map/ppermute | solution.py:484
  26.2 1.6 %collective-permute-start.9 = (bf16[96,1152]{1,0:T(8,128)(2,1)S(1)}, bf16[96,1152]{1,0:T(8,128)(2,1)S(1)}, u32[]{:S(2)}, u32[]{:S(2)}) collective-permute-start(bf16[96,1152]{1,0:T(8,128)(2,1)S(1)} %constant_dynamic-update-slice_fusion.refs_0_.column), channel_id=1, source_target_pairs={{0,4},{2,6},{4,0},{6,2},{8,12},{10,14},{12,8},{14,10},{16,20},{18,... | collective-permute-start | bytes 663560 | tf_op jit(solution)/shard_map/ppermute | solution.py:484
  27.8 1.5 %collective-permute-start.10 = (bf16[96,1152]{1,0:T(8,128)(2,1)S(1)}, bf16[96,1152]{1,0:T(8,128)(2,1)S(1)}, u32[]{:S(2)}, u32[]{:S(2)}) collective-permute-start(bf16[96,1152]{1,0:T(8,128)(2,1)S(1)} %constant_dynamic-update-slice_fusion.refs_0_.column), channel_id=1, source_target_pairs={{0,2},{2,0},{4,6},{6,4},{8,10},{10,8},{12,14},{14,12},{16,18},{18,... | collective-permute-start | bytes 663560 | tf_op jit(solution)/shard_map/ppermute | solution.py:484
  29.3 0.5 collective-permute-start.4
  29.7 3.9 %collective-permute-done.9.refs_0_ = bf16[96,1152]{1,0:T(8,128)(2,1)S(1)} collective-permute-done((bf16[96,1152]{1,0:T(8,128)(2,1)S(1)}, bf16[96,1152]{1,0:T(8,128)(2,1)S(1)}, u32[]{:S(2)}, u32[]{:S(2)}) %collective-permute-start.9) | collective-permute-done | bytes 221216 | tf_op jit(solution)/shard_map/ppermute | solution.py:484
  33.6 0.0 collective-permute-start.11
  33.6 2.3 %collective-permute-done.10.refs_1_ = bf16[96,1152]{1,0:T(8,128)(2,1)S(1)} collective-permute-done((bf16[96,1152]{1,0:T(8,128)(2,1)S(1)}, bf16[96,1152]{1,0:T(8,128)(2,1)S(1)}, u32[]{:S(2)}, u32[]{:S(2)}) %collective-permute-start.10) | collective-permute-done | bytes 221216 | tf_op jit(solution)/shard_map/ppermute | solution.py:484
  35.9 0.0 collective-permute-start.12
  36.0 0.5 collective-permute-start.5
  36.5 1.8 %collective-permute-done.4.refs_1_ = bf16[96,1152]{1,0:T(8,128)(2,1)S(1)} collective-permute-done((bf16[96,1152]{1,0:T(8,128)(2,1)S(1)}, bf16[96,1152]{1,0:T(8,128)(2,1)S(1)}, u32[]{:S(2)}, u32[]{:S(2)}) %collective-permute-start.4) | collective-permute-done | bytes 221216 | tf_op jit(solution)/shard_map/ppermute | solution.py:484
  38.3 0.0 collective-permute-start.6
  38.3 0.0 collective-permute-done.11.refs_2_
  38.3 0.0 collective-permute-done.12.refs_3_
  38.3 2.5 %shard_map.261 = (bf16[248,512]{1,0:T(8,128)(2,1)S(1)}, f32[48,128]{1,0:T(8,128)S(1)}) custom-call(s32[6]{0:T(128)S(1)} %pad_add_fusion.ids, bf16[96,1152]{1,0:T(8,128)(2,1)S(1)} %collective-permute-done.9.refs_0_, bf16[96,1152]{1,0:T(8,128)(2,1)S(1)} %collective-permute-done.10.refs_1_, bf16[96,1152]{1,0:T(8,128)(2,1)S(1)} %collective-permute-done.11.refs_2_, ...), custom_call_target="tpu_custom_call" | custom-call | tf_op jit(solution)/shard_map/pallas_call | solution.py:61
  40.7 0.6 collective-permute-start.13
  41.3 0.0 collective-permute-done.5.refs_2_
  41.3 0.0 collective-permute-done.6.refs_3_
  41.3 2.5 %shard_map.258 = (bf16[248,512]{1,0:T(8,128)(2,1)S(1)}, f32[48,128]{1,0:T(8,128)S(1)}) custom-call(s32[6]{0:T(128)S(1)} %pad_add_fusion.ids, bf16[96,1152]{1,0:T(8,128)(2,1)S(1)} %constant_dynamic-update-slice_fusion.refs_0_.column, bf16[96,1152]{1,0:T(8,128)(2,1)S(1)} %collective-permute-done.4.refs_1_, ...), custom_call_target="tpu_custom_call" | custom-call | tf_op jit(solution)/shard_map/pallas_call | solution.py:61
  43.8 0.1 collective-permute-start.7
  43.9 2.1 %shard_map.259 = (bf16[512,1024]{1,0:T(8,128)(2,1)S(1)}, bf16[512,1024]{1,0:T(8,128)(2,1)S(1)}) custom-call(s32[6]{0:T(128)S(1)} %pad_add_fusion.ids, bf16[96,1152]{1,0:T(8,128)(2,1)S(1)} %constant_dynamic-update-slice_fusion.refs_0_.column, bf16[512,2048]{1,0:T(8,128)(2,1)} %down_in.3, bf16[512,2048]{1,0:T(8,128)(2,1)} %bitcast.13), custom_call_target="tpu_custom_call" | custom-call | tf_op jit(solution)/shard_map/pallas_call | solution.py:61
  46.0 0.0 collective-permute-done.8.down_got
  46.0 0.9 %shard_map.262 = (bf16[128,1024]{1,0:T(8,128)(2,1)S(1)}, bf16[128,1024]{1,0:T(8,128)(2,1)S(1)}) custom-call(bf16[248,512]{1,0:T(8,128)(2,1)S(1)} %get-tuple-element.42.own, bf16[248,512]{1,0:T(8,128)(2,1)S(1)} %collective-permute-done.13.other, bf16[512,1024]{1,0:T(8,128)(2,1)S(1)} %get-tuple-element.37.down_own, ...), custom_call_target="tpu_custom_call" | custom-call | tf_op jit(solution)/shard_map/pallas_call | solution.py:61
  46.9 1.6 %collective-permute-start.14 = (bf16[128,1024]{1,0:T(8,128)(2,1)S(1)}, bf16[128,1024]{1,0:T(8,128)(2,1)S(1)}, u32[]{:S(2)}, u32[]{:S(2)}) collective-permute-start(bf16[128,1024]{1,0:T(8,128)(2,1)S(1)} %get-tuple-element.44), channel_id=1, source_target_pairs={{0,2},{2,0},{4,6},{6,4},{8,10},{10,8},{12,14},{14,12},{16,18},{18,... | collective-permute-start | bytes 786440 | tf_op jit(solution)/shard_map/ppermute | solution.py:484
  48.5 1.5 %collective-permute-start.15 = (bf16[128,1024]{1,0:T(8,128)(2,1)S(1)}, bf16[128,1024]{1,0:T(8,128)(2,1)S(1)}, u32[]{:S(2)}, u32[]{:S(2)}) collective-permute-start(bf16[128,1024]{1,0:T(8,128)(2,1)S(1)} %get-tuple-element.45), channel_id=1, source_target_pairs={{0,4},{2,6},{4,0},{6,2},{8,12},{10,14},{12,8},{14,10},{16,20},{18,... | collective-permute-start | bytes 786440 | tf_op jit(solution)/shard_map/ppermute | solution.py:484
  50.0 0.0 collective-permute-done.7.other
  50.0 0.9 %shard_map.260 = (bf16[128,1024]{1,0:T(8,128)(2,1)S(1)}, bf16[128,1024]{1,0:T(8,128)(2,1)S(1)}) custom-call(bf16[248,512]{1,0:T(8,128)(2,1)S(1)} %get-tuple-element.36.own, bf16[248,512]{1,0:T(8,128)(2,1)S(1)} %collective-permute-done.7.other, bf16[512,1024]{1,0:T(8,128)(2,1)S(1)} %get-tuple-element.37.down_own, ...), custom_call_target="tpu_custom_call" | custom-call | tf_op jit(solution)/shard_map/pallas_call | solution.py:61
  50.9 0.5 collective-permute-start.16
  51.5 0.6 copy.61
  52.1 0.6 copy.62
  52.7 0.7 copy.56
  53.3 0.8 %shard_map.263.refs_4_ = bf16[4,64,24]{2,1,0:T(8,128)(2,1)S(1)} custom-call(s32[6]{0:T(128)S(1)} %pad_add_fusion.ids, bf16[96,1152]{1,0:T(8,128)(2,1)S(1)} %constant_dynamic-update-slice_fusion.refs_0_.column), custom_call_target="tpu_custom_call" | custom-call | tf_op jit(solution)/shard_map/pallas_call | solution.py:61
  54.1 2.1 %collective-permute-done.14.refs_1_ = bf16[128,1024]{1,0:T(8,128)(2,1)S(1)} collective-permute-done((bf16[128,1024]{1,0:T(8,128)(2,1)S(1)}, bf16[128,1024]{1,0:T(8,128)(2,1)S(1)}, u32[]{:S(2)}, u32[]{:S(2)}) %collective-permute-start.14) | collective-permute-done | bytes 262176 | tf_op jit(solution)/shard_map/ppermute | solution.py:484
  56.2 6.4 %collective-permute-done.15.refs_2_ = bf16[128,1024]{1,0:T(8,128)(2,1)S(1)} collective-permute-done((bf16[128,1024]{1,0:T(8,128)(2,1)S(1)}, bf16[128,1024]{1,0:T(8,128)(2,1)S(1)}, u32[]{:S(2)}, u32[]{:S(2)}) %collective-permute-start.15) | collective-permute-done | bytes 262176 | tf_op jit(solution)/shard_map/ppermute | solution.py:484
  62.5 0.0 collective-permute-done.16.refs_3_
  62.5 0.3 shard_map.264
  62.8 0.2 collective-permute-start.17
  63.0 1.6 %collective-permute-start.18 = (bf16[40,1024]{1,0:T(8,128)(2,1)S(1)}, bf16[40,1024]{1,0:T(8,128)(2,1)S(1)}, u32[]{:S(2)}, u32[]{:S(2)}) collective-permute-start(bf16[40,1024]{1,0:T(8,128)(2,1)S(1)} %get-tuple-element.49), channel_id=1, source_target_pairs={{0,16},{2,18},{4,20},{6,22},{8,24},{10,26},{12,28},{14,30},{16,0},... | collective-permute-start | bytes 245768 | tf_op jit(solution)/shard_map/ppermute | solution.py:484
  64.6 2.7 %collective-permute-start.19 = (bf16[40,1024]{1,0:T(8,128)(2,1)S(1)}, bf16[40,1024]{1,0:T(8,128)(2,1)S(1)}, u32[]{:S(2)}, u32[]{:S(2)}) collective-permute-start(bf16[40,1024]{1,0:T(8,128)(2,1)S(1)} %get-tuple-element.50), channel_id=1, source_target_pairs={{0,24},{2,26},{4,28},{6,30},{8,16},{10,18},{12,20},{14,22},{16,8},... | collective-permute-start | bytes 245768 | tf_op jit(solution)/shard_map/ppermute | solution.py:484
  67.3 0.3 collective-permute-done.17.refs_2_
  67.6 4.6 %collective-permute-done.18.refs_3_ = bf16[40,1024]{1,0:T(8,128)(2,1)S(1)} collective-permute-done((bf16[40,1024]{1,0:T(8,128)(2,1)S(1)}, bf16[40,1024]{1,0:T(8,128)(2,1)S(1)}, u32[]{:S(2)}, u32[]{:S(2)}) %collective-permute-start.18) | collective-permute-done | bytes 81952 | tf_op jit(solution)/shard_map/ppermute | solution.py:484
  72.2 0.0 collective-permute-done.19.refs_4_
  72.2 0.8 %shard_map.265 = bf16[24,1024]{1,0:T(8,128)(2,1)S(1)} custom-call(s32[4]{0:T(128)S(1)} %iota_xor_fusion.refs_0_, bf16[40,1024]{1,0:T(8,128)(2,1)S(1)} %get-tuple-element.47.refs_1_, bf16[40,1024]{1,0:T(8,128)(2,1)S(1)} %collective-permute-done.17.refs_2_, bf16[40,1024]{1,0:T(8,128)(2,1)S(1)} %collective-permute-done.18.refs_3_, ...), custom_call_target="tpu_custom_call" | custom-call | tf_op jit(solution)/shard_map/pallas_call | solution.py:61
  73.0 0.6 copy.60
  (19 shorter events, 0.1 us)
Async XLA Ops:
  0.7 7.3 %copy-start.3 = (s32[24,2]{0,1:T(2,128)S(1)}, s32[24,2]{0,1:T(2,128)}, u32[]{:S(2)}) copy-start(s32[24,2]{0,1:T(2,128)} %param.43) | copy-start | bytes 580
  0.8 7.4 %copy-start.4 = (f32[24,2]{0,1:T(2,128)S(1)}, f32[24,2]{0,1:T(2,128)}, u32[]{:S(2)}) copy-start(f32[24,2]{0,1:T(2,128)} %param.44) | copy-start | bytes 580
  0.8 8.2 %copy-start = (bf16[24,2048]{1,0:T(8,128)(2,1)S(1)}, bf16[24,2048]{1,0:T(8,128)(2,1)}, u32[]{:S(2)}) copy-start(bf16[24,2048]{1,0:T(8,128)(2,1)} %tokens.1) | copy-start | bytes 294916
  0.8 8.2 %copy-start.1 = (bf16[2048]{0:T(1024)(128)(2,1)S(1)}, bf16[2048]{0:T(1024)(128)(2,1)}, u32[]{:S(2)}) copy-start(bf16[2048]{0:T(1024)(128)(2,1)} %gain.1) | copy-start | bytes 12292
  0.8 8.2 %copy-start.2 = (bf16[2048]{0:T(1024)(128)(2,1)S(1)}, bf16[2048]{0:T(1024)(128)(2,1)}, u32[]{:S(2)}) copy-start(bf16[2048]{0:T(1024)(128)(2,1)} %branch_gate.1) | copy-start | bytes 12292
  7.5 1.5 %collective-permute-start = (bf16[24,2048]{1,0:T(8,128)(2,1)S(1)}, bf16[24,2048]{1,0:T(8,128)(2,1)S(1)}, u32[]{:S(2)}, u32[]{:S(2)}) collective-permute-start(bf16[24,2048]{1,0:T(8,128)(2,1)S(1)} %get-tuple-element.30.part_a), channel_id=1, source_target_pairs={{0,1},{1,0},{2,3},{3,2},{4,5},{5,4},{6,7},{7,6},{8,9},{9,8},{10,11... | collective-permute-start | bytes 294920 | tf_op jit(solution)/shard_map/ppermute | solution.py:481
  14.5 31.5 %collective-permute-start.8 = (bf16[1024,1024]{1,0:T(8,128)(2,1)S(1)}, bf16[1024,1024]{1,0:T(8,128)(2,1)S(1)}, u32[]{:S(2)}, u32[]{:S(2)}) collective-permute-start(bf16[1024,1024]{1,0:T(8,128)(2,1)S(1)} %get-tuple-element.39), channel_id=1, source_target_pairs={{0,1},{1,0},{2,3},{3,2},{4,5},{5,4},{6,7},{7,6},{8,9},{9,8},{10,11... | collective-permute-start | bytes 6291464 | tf_op jit(solution)/shard_map/ppermute | solution.py:481
  14.9 5.3 %collective-permute-start.1 = (bf16[24,1152]{1,0:T(8,128)(2,1)S(1)}, bf16[24,1152]{1,0:T(8,128)(2,1)S(1)}, u32[]{:S(2)}, u32[]{:S(2)}) collective-permute-start(bf16[24,1152]{1,0:T(8,128)(2,1)S(1)} %get-tuple-element.31.anchor), channel_id=1, source_target_pairs={{0,8},{2,10},{4,12},{6,14},{8,0},{10,2},{12,4},{14,6},{16,24},{18,... | collective-permute-start | bytes 165896 | tf_op jit(solution)/shard_map/ppermute | solution.py:484
  17.6 6.4 %collective-permute-start.2 = (bf16[24,1152]{1,0:T(8,128)(2,1)S(1)}, bf16[24,1152]{1,0:T(8,128)(2,1)S(1)}, u32[]{:S(2)}, u32[]{:S(2)}) collective-permute-start(bf16[24,1152]{1,0:T(8,128)(2,1)S(1)} %get-tuple-element.31.anchor), channel_id=1, source_target_pairs={{0,16},{2,18},{4,20},{6,22},{8,24},{10,26},{12,28},{14,30},{16,0},... | collective-permute-start | bytes 165896 | tf_op jit(solution)/shard_map/ppermute | solution.py:484
  20.2 6.0 %collective-permute-start.3 = (bf16[24,1152]{1,0:T(8,128)(2,1)S(1)}, bf16[24,1152]{1,0:T(8,128)(2,1)S(1)}, u32[]{:S(2)}, u32[]{:S(2)}) collective-permute-start(bf16[24,1152]{1,0:T(8,128)(2,1)S(1)} %get-tuple-element.31.anchor), channel_id=1, source_target_pairs={{0,24},{2,26},{4,28},{6,30},{8,16},{10,18},{12,20},{14,22},{16,8},... | collective-permute-start | bytes 165896 | tf_op jit(solution)/shard_map/ppermute | solution.py:484
  26.2 7.5 %collective-permute-start.9 = (bf16[96,1152]{1,0:T(8,128)(2,1)S(1)}, bf16[96,1152]{1,0:T(8,128)(2,1)S(1)}, u32[]{:S(2)}, u32[]{:S(2)}) collective-permute-start(bf16[96,1152]{1,0:T(8,128)(2,1)S(1)} %constant_dynamic-update-slice_fusion.refs_0_.column), channel_id=1, source_target_pairs={{0,4},{2,6},{4,0},{6,2},{8,12},{10,14},{12,8},{14,10},{16,20},{18,... | collective-permute-start | bytes 663560 | tf_op jit(solution)/shard_map/ppermute | solution.py:484
  27.8 8.2 %collective-permute-start.10 = (bf16[96,1152]{1,0:T(8,128)(2,1)S(1)}, bf16[96,1152]{1,0:T(8,128)(2,1)S(1)}, u32[]{:S(2)}, u32[]{:S(2)}) collective-permute-start(bf16[96,1152]{1,0:T(8,128)(2,1)S(1)} %constant_dynamic-update-slice_fusion.refs_0_.column), channel_id=1, source_target_pairs={{0,2},{2,0},{4,6},{6,4},{8,10},{10,8},{12,14},{14,12},{16,18},{18,... | collective-permute-start | bytes 663560 | tf_op jit(solution)/shard_map/ppermute | solution.py:484
  29.3 9.0 %collective-permute-start.4 = (bf16[96,1152]{1,0:T(8,128)(2,1)S(1)}, bf16[96,1152]{1,0:T(8,128)(2,1)S(1)}, u32[]{:S(2)}, u32[]{:S(2)}) collective-permute-start(bf16[96,1152]{1,0:T(8,128)(2,1)S(1)} %constant_dynamic-update-slice_fusion.refs_0_.column), channel_id=1, source_target_pairs={{0,6},{2,4},{4,2},{6,0},{8,14},{10,12},{12,10},{14,8},{16,22},{18,... | collective-permute-start | bytes 663560 | tf_op jit(solution)/shard_map/ppermute | solution.py:484
  33.6 4.6 %collective-permute-start.11 = (bf16[96,1152]{1,0:T(8,128)(2,1)S(1)}, bf16[96,1152]{1,0:T(8,128)(2,1)S(1)}, u32[]{:S(2)}, u32[]{:S(2)}) collective-permute-start(bf16[96,1152]{1,0:T(8,128)(2,1)S(1)} %collective-permute-done.9.refs_0_), channel_id=1, source_target_pairs={{0,1},{1,0},{2,3},{3,2},{4,5},{5,4},{6,7},{7,6},{8,9},{9,8},{10,11... | collective-permute-start | bytes 663560 | tf_op jit(solution)/shard_map/ppermute | solution.py:481
  35.9 2.3 %collective-permute-start.12 = (bf16[96,1152]{1,0:T(8,128)(2,1)S(1)}, bf16[96,1152]{1,0:T(8,128)(2,1)S(1)}, u32[]{:S(2)}, u32[]{:S(2)}) collective-permute-start(bf16[96,1152]{1,0:T(8,128)(2,1)S(1)} %collective-permute-done.10.refs_1_), channel_id=1, source_target_pairs={{0,1},{1,0},{2,3},{3,2},{4,5},{5,4},{6,7},{7,6},{8,9},{9,8},{10,11... | collective-permute-start | bytes 663560 | tf_op jit(solution)/shard_map/ppermute | solution.py:481
  36.0 5.4 %collective-permute-start.5 = (bf16[96,1152]{1,0:T(8,128)(2,1)S(1)}, bf16[96,1152]{1,0:T(8,128)(2,1)S(1)}, u32[]{:S(2)}, u32[]{:S(2)}) collective-permute-start(bf16[96,1152]{1,0:T(8,128)(2,1)S(1)} %constant_dynamic-update-slice_fusion.refs_0_.column), channel_id=1, source_target_pairs={{0,1},{1,0},{2,3},{3,2},{4,5},{5,4},{6,7},{7,6},{8,9},{9,8},{10,11... | collective-permute-start | bytes 663560 | tf_op jit(solution)/shard_map/ppermute | solution.py:481
  38.3 3.1 %collective-permute-start.6 = (bf16[96,1152]{1,0:T(8,128)(2,1)S(1)}, bf16[96,1152]{1,0:T(8,128)(2,1)S(1)}, u32[]{:S(2)}, u32[]{:S(2)}) collective-permute-start(bf16[96,1152]{1,0:T(8,128)(2,1)S(1)} %collective-permute-done.4.refs_1_), channel_id=1, source_target_pairs={{0,1},{1,0},{2,3},{3,2},{4,5},{5,4},{6,7},{7,6},{8,9},{9,8},{10,11... | collective-permute-start | bytes 663560 | tf_op jit(solution)/shard_map/ppermute | solution.py:481
  40.7 5.3 %collective-permute-start.13 = (bf16[248,512]{1,0:T(8,128)(2,1)S(1)}, bf16[248,512]{1,0:T(8,128)(2,1)S(1)}, u32[]{:S(2)}, u32[]{:S(2)}) collective-permute-start(bf16[248,512]{1,0:T(8,128)(2,1)S(1)} %get-tuple-element.42.own), channel_id=1, source_target_pairs={{0,1},{1,0},{2,3},{3,2},{4,5},{5,4},{6,7},{7,6},{8,9},{9,8},{10,11... | collective-permute-start | bytes 761864 | tf_op jit(solution)/shard_map/ppermute | solution.py:481
  43.8 6.2 %collective-permute-start.7 = (bf16[248,512]{1,0:T(8,128)(2,1)S(1)}, bf16[248,512]{1,0:T(8,128)(2,1)S(1)}, u32[]{:S(2)}, u32[]{:S(2)}) collective-permute-start(bf16[248,512]{1,0:T(8,128)(2,1)S(1)} %get-tuple-element.36.own), channel_id=1, source_target_pairs={{0,1},{1,0},{2,3},{3,2},{4,5},{5,4},{6,7},{7,6},{8,9},{9,8},{10,11... | collective-permute-start | bytes 761864 | tf_op jit(solution)/shard_map/ppermute | solution.py:481
  46.9 9.2 %collective-permute-start.14 = (bf16[128,1024]{1,0:T(8,128)(2,1)S(1)}, bf16[128,1024]{1,0:T(8,128)(2,1)S(1)}, u32[]{:S(2)}, u32[]{:S(2)}) collective-permute-start(bf16[128,1024]{1,0:T(8,128)(2,1)S(1)} %get-tuple-element.44), channel_id=1, source_target_pairs={{0,2},{2,0},{4,6},{6,4},{8,10},{10,8},{12,14},{14,12},{16,18},{18,... | collective-permute-start | bytes 786440 | tf_op jit(solution)/shard_map/ppermute | solution.py:484
  48.5 14.0 %collective-permute-start.15 = (bf16[128,1024]{1,0:T(8,128)(2,1)S(1)}, bf16[128,1024]{1,0:T(8,128)(2,1)S(1)}, u32[]{:S(2)}, u32[]{:S(2)}) collective-permute-start(bf16[128,1024]{1,0:T(8,128)(2,1)S(1)} %get-tuple-element.45), channel_id=1, source_target_pairs={{0,4},{2,6},{4,0},{6,2},{8,12},{10,14},{12,8},{14,10},{16,20},{18,... | collective-permute-start | bytes 786440 | tf_op jit(solution)/shard_map/ppermute | solution.py:484
  50.9 11.6 %collective-permute-start.16 = (bf16[128,1024]{1,0:T(8,128)(2,1)S(1)}, bf16[128,1024]{1,0:T(8,128)(2,1)S(1)}, u32[]{:S(2)}, u32[]{:S(2)}) collective-permute-start(bf16[128,1024]{1,0:T(8,128)(2,1)S(1)} %get-tuple-element.46), channel_id=1, source_target_pairs={{0,6},{2,4},{4,2},{6,0},{8,14},{10,12},{12,10},{14,8},{16,22},{18,... | collective-permute-start | bytes 786440 | tf_op jit(solution)/shard_map/ppermute | solution.py:484
  62.8 4.8 %collective-permute-start.17 = (bf16[40,1024]{1,0:T(8,128)(2,1)S(1)}, bf16[40,1024]{1,0:T(8,128)(2,1)S(1)}, u32[]{:S(2)}, u32[]{:S(2)}) collective-permute-start(bf16[40,1024]{1,0:T(8,128)(2,1)S(1)} %get-tuple-element.48), channel_id=1, source_target_pairs={{0,8},{2,10},{4,12},{6,14},{8,0},{10,2},{12,4},{14,6},{16,24},{18,... | collective-permute-start | bytes 245768 | tf_op jit(solution)/shard_map/ppermute | solution.py:484
  63.0 9.2 %collective-permute-start.18 = (bf16[40,1024]{1,0:T(8,128)(2,1)S(1)}, bf16[40,1024]{1,0:T(8,128)(2,1)S(1)}, u32[]{:S(2)}, u32[]{:S(2)}) collective-permute-start(bf16[40,1024]{1,0:T(8,128)(2,1)S(1)} %get-tuple-element.49), channel_id=1, source_target_pairs={{0,16},{2,18},{4,20},{6,22},{8,24},{10,26},{12,28},{14,30},{16,0},... | collective-permute-start | bytes 245768 | tf_op jit(solution)/shard_map/ppermute | solution.py:484
  64.6 7.6 %collective-permute-start.19 = (bf16[40,1024]{1,0:T(8,128)(2,1)S(1)}, bf16[40,1024]{1,0:T(8,128)(2,1)S(1)}, u32[]{:S(2)}, u32[]{:S(2)}) collective-permute-start(bf16[40,1024]{1,0:T(8,128)(2,1)S(1)} %get-tuple-element.50), channel_id=1, source_target_pairs={{0,24},{2,26},{4,28},{6,30},{8,16},{10,18},{12,20},{14,22},{16,8},... | collective-permute-start | bytes 245768 | tf_op jit(solution)/shard_map/ppermute | solution.py:484

commit v3 on v2

--- a/solution.py
+++ b/solution.py
@@ -216,17 +216,21 @@
     out[count : count + slots, 0 : expert_gate.shape[1]] = active.astype(BF16)
 
 
-def down_kernel(own, other, down_own, expert_own, down_got, slot_weight, *outs, count):
+def base_kernel(own, down_own, expert_own, dense, routed):
+    count, slots = dense.shape[0], routed.shape[0]
+    dense[...] = dot(own[0:count, 0 : down_own.shape[0]], down_own[...])
+    routed[...] = dot(own[count : count + slots, 0 : expert_own.shape[0]], expert_own[...])
+
+
+def down_kernel(own, other, dense_base, routed_base, down_got, slot_weight, *outs, hidden):
     plane = len(outs)
     half = outs[0].shape[1]
+    count = dense_base.shape[0]
     slots = slot_weight.shape[0]
-    hidden, routed_hidden = down_own.shape[0], expert_own.shape[0]
-    dense = dot(own[0:count, 0:hidden], down_own[...]) + dot(
-        other[0:count, 0:hidden], down_got[0:hidden, :]
-    )
-    routed_rows = slice(count, count + slots)
-    routed = dot(own[routed_rows, 0:routed_hidden], expert_own[...]) + dot(
-        other[routed_rows, 0:routed_hidden], down_got[hidden:, :]
+    routed_hidden = down_got.shape[0] - hidden
+    dense = dense_base[...] + dot(other[0:count, 0:hidden], down_got[0:hidden, :])
+    routed = routed_base[...] + dot(
+        other[count : count + slots, 0:routed_hidden], down_got[hidden:, :]
     )
     routed = routed * slot_weight[:, 0:1]
     squares = own[count + slots :, 0:LANES].astype(F32) + other[count + slots :, 0:LANES].astype(F32)
@@ -551,10 +555,15 @@
             ],
         )
         hidden_other = swap(hidden)
+        dense_base, routed_base = call(
+            base_kernel,
+            [((rows, half), F32), ((routes, half), F32)],
+            [hidden, down_own, expert_own],
+        )
         sums = call(
-            functools.partial(down_kernel, count=rows),
+            functools.partial(down_kernel, hidden=ff_local),
             [((planes * (seq + capacity) + 8, half), BF16)] * size,
-            [hidden, hidden_other, down_own, expert_own, down_got, slot_weight],
+            [hidden, hidden_other, dense_base, routed_base, down_got, slot_weight],
         )
         for j, value in zip(members, sums):
             arrived[j] = exchange(value, j) if j else value

time: 73.8 us -> 75.1 us (1.018)
  waiting for transfers between devices: 27.4 us -> 28.5 us
    ppermute x8, waiting for transfers between devices: 0.14 us -> 1.08 us  [swap(): return lax.ppermute(values, 'tp', [(i, 1 - i) for i in range(tp_count)])]
    pallas_call x11 -> x13, Pallas kernels: 22.9 us -> 23.2 us  [call(): pl.pallas_call(kernel, in_specs=specs, out_specs=[VMEM] * len(outs), out_...]
where the time goes in v3:
time: 75.1 us; the launch traced here: 75 us
  waiting for transfers between devices  28.5 us (38%)
  Pallas kernels  23.2 us (31%)
  starting transfers between devices  19.1 us (25%)
  local copies, waits for them, and re-layouts  3.1 us (4%)
  between operations  0.84 us (1%)
    ppermute x12, waiting for transfers between devices, exchange(): return lax.ppermute(values, 'ep', [(i, i ^ mask) for i in range(ep_count)])  27.4 us
    pallas_call x13, Pallas kernels, call(): pl.pallas_call(kernel, in_specs=specs, out_specs=[VMEM] * len(outs), out_...  23.2 us
    ppermute x12, starting transfers between devices, exchange(): return lax.ppermute(values, 'ep', [(i, i ^ mask) for i in range(ep_count)])  16.9 us
    unnamed x18, local copies, waits for them, and re-layouts  2.6 us
    ppermute x8, starting transfers between devices, swap(): return lax.ppermute(values, 'tp', [(i, 1 - i) for i in range(tp_count)])  2.14 us
  transfers between devices with their start and end apart: 20, of which 10 were waited for; matrix products, arithmetic and copies ran while one was open for 4% of the time, Pallas kernels for 13%

profile of v3, /device:TPU:0, one launch (start us, length us, event | category | flops | bytes accessed | tf_op | source)
XLA Modules:
  0.0 75.0 jit_solution(8313799104136046190)
XLA Ops:
  0.7 0.1 pad_add_fusion.ids
  0.8 0.0 copy-start.2
  0.8 6.7 %shard_map.255 = (bf16[24,2048]{1,0:T(8,128)(2,1)S(1)}, bf16[24,64]{1,0:T(8,128)(2,1)S(1)}, bf16[24,64]{1,0:T(8,128)(2,1)S(1)}, f32[24,8]{1,0:T(8,128)S(1)}) custom-call(s32[6]{0:T(128)S(1)} %pad_add_fusion.ids, s32[24]{0:T(128)} %lens_in.1, bf16[24,2048]{1,0:T(8,128)(2,1)} %tokens.1, bf16[2048]{0:T(1024)(128)(2,1)} %norm_in.1, bf16[64]{0:T(256)(128)(2,1)} %query_in.1, ...), custom_call_target="tpu_custom_call" | custom-call | tf_op jit(solution)/shard_map/pallas_call | solution.py:61
  7.5 0.6 collective-permute-start
  8.1 0.1 copy.52
  8.1 0.1 copy.55
  8.2 0.1 copy.54
  8.3 0.1 copy.53
  8.4 0.1 eq.17
  8.5 0.1 fusion
  8.7 0.1 reduce_sum.12
  8.8 0.1 fusion.5.notes.refs_7_
  8.9 0.1 collective-permute-done.part_b
  9.0 0.8 %shard_map.256 = (bf16[24,1152]{1,0:T(8,128)(2,1)S(1)}, bf16[24,1024]{1,0:T(8,128)(2,1)S(1)}, f32[24,128]{1,0:T(8,128)S(1)}) custom-call(s32[6]{0:T(128)S(1)} %pad_add_fusion.ids, bf16[24,2048]{1,0:T(8,128)(2,1)S(1)} %copy-done, bf16[24,2048]{1,0:T(8,128)(2,1)S(1)} %get-tuple-element.34.part_a, bf16[24,2048]{1,0:T(8,128)(2,1)S(1)} %collective-permute-done.part_b, ...), custom_call_target="tpu_custom_call" | custom-call | tf_op jit(solution)/shard_map/pallas_call | solution.py:61
  9.8 4.7 %shard_map.257 = (bf16[1024,1024]{1,0:T(8,128)(2,1)S(1)}, bf16[2048,512]{1,0:T(8,128)(2,1)S(1)}, bf16[2048,512]{1,0:T(8,128)(2,1)S(1)}, bf16[2048,512]{1,0:T(8,128)(2,1)S(1)}, bf16[2048,512]{1,0:T(8,128)(2,1)S(1)}) custom-call(s32[6]{0:T(128)S(1)} %pad_add_fusion.ids, bf16[24,1152]{1,0:T(8,128)(2,1)S(1)} %get-tuple-element.35.anchor, ...), custom_call_target="tpu_custom_call" | custom-call | tf_op jit(solution)/shard_map/pallas_call | solution.py:61
  14.5 0.4 collective-permute-start.8
  14.9 4.7 %collective-permute-start.3 = (bf16[24,1152]{1,0:T(8,128)(2,1)S(1)}, bf16[24,1152]{1,0:T(8,128)(2,1)S(1)}, u32[]{:S(2)}, u32[]{:S(2)}) collective-permute-start(bf16[24,1152]{1,0:T(8,128)(2,1)S(1)} %get-tuple-element.35.anchor), channel_id=1, source_target_pairs={{0,24},{2,26},{4,28},{6,30},{8,16},{10,18},{12,20},{14,22},{16,8},... | collective-permute-start | bytes 165896 | tf_op jit(solution)/shard_map/ppermute | solution.py:488
  19.7 0.0 collective-permute-start.2
  19.7 0.6 collective-permute-start.1
  20.2 4.8 %collective-permute-done.1 = bf16[24,1152]{1,0:T(8,128)(2,1)S(1)} collective-permute-done((bf16[24,1152]{1,0:T(8,128)(2,1)S(1)}, bf16[24,1152]{1,0:T(8,128)(2,1)S(1)}, u32[]{:S(2)}, u32[]{:S(2)}) %collective-permute-start.1) | collective-permute-done | bytes 55328 | tf_op jit(solution)/shard_map/ppermute | solution.py:488
  25.0 0.0 collective-permute-done.2
  25.0 0.0 collective-permute-done.3
  25.1 1.6 %collective-permute-start.10 = (bf16[96,1152]{1,0:T(8,128)(2,1)S(1)}, bf16[96,1152]{1,0:T(8,128)(2,1)S(1)}, u32[]{:S(2)}, u32[]{:S(2)}) collective-permute-start(bf16[96,1152]{1,0:T(8,128)(2,1)S(1)} %constant_dynamic-update-slice_fusion.refs_0_.column), channel_id=1, source_target_pairs={{0,2},{2,0},{4,6},{6,4},{8,10},{10,8},{12,14},{14,12},{16,18},{18,... | collective-permute-start | bytes 663560 | tf_op jit(solution)/shard_map/ppermute | solution.py:488
  26.6 1.5 %collective-permute-start.9 = (bf16[96,1152]{1,0:T(8,128)(2,1)S(1)}, bf16[96,1152]{1,0:T(8,128)(2,1)S(1)}, u32[]{:S(2)}, u32[]{:S(2)}) collective-permute-start(bf16[96,1152]{1,0:T(8,128)(2,1)S(1)} %constant_dynamic-update-slice_fusion.refs_0_.column), channel_id=1, source_target_pairs={{0,4},{2,6},{4,0},{6,2},{8,12},{10,14},{12,8},{14,10},{16,20},{18,... | collective-permute-start | bytes 663560 | tf_op jit(solution)/shard_map/ppermute | solution.py:488
  28.1 0.5 collective-permute-start.4
  28.6 4.8 %collective-permute-done.10.refs_1_ = bf16[96,1152]{1,0:T(8,128)(2,1)S(1)} collective-permute-done((bf16[96,1152]{1,0:T(8,128)(2,1)S(1)}, bf16[96,1152]{1,0:T(8,128)(2,1)S(1)}, u32[]{:S(2)}, u32[]{:S(2)}) %collective-permute-start.10) | collective-permute-done | bytes 221216 | tf_op jit(solution)/shard_map/ppermute | solution.py:488
  33.4 0.0 collective-permute-start.12
  33.4 4.5 %collective-permute-done.9.refs_0_ = bf16[96,1152]{1,0:T(8,128)(2,1)S(1)} collective-permute-done((bf16[96,1152]{1,0:T(8,128)(2,1)S(1)}, bf16[96,1152]{1,0:T(8,128)(2,1)S(1)}, u32[]{:S(2)}, u32[]{:S(2)}) %collective-permute-start.9) | collective-permute-done | bytes 221216 | tf_op jit(solution)/shard_map/ppermute | solution.py:488
  38.0 0.0 collective-permute-start.11
  38.0 0.5 collective-permute-start.5
  38.5 0.0 collective-permute-done.4.refs_1_
  38.5 0.0 collective-permute-start.6
  38.5 0.0 collective-permute-done.12.refs_3_
  38.5 1.0 %collective-permute-done.11.refs_2_ = bf16[96,1152]{1,0:T(8,128)(2,1)S(1)} collective-permute-done((bf16[96,1152]{1,0:T(8,128)(2,1)S(1)}, bf16[96,1152]{1,0:T(8,128)(2,1)S(1)}, u32[]{:S(2)}, u32[]{:S(2)}) %collective-permute-start.11) | collective-permute-done | bytes 221216 | tf_op jit(solution)/shard_map/ppermute | solution.py:485
  39.4 2.5 %shard_map.262 = (bf16[248,512]{1,0:T(8,128)(2,1)S(1)}, f32[48,128]{1,0:T(8,128)S(1)}) custom-call(s32[6]{0:T(128)S(1)} %pad_add_fusion.ids, bf16[96,1152]{1,0:T(8,128)(2,1)S(1)} %collective-permute-done.9.refs_0_, bf16[96,1152]{1,0:T(8,128)(2,1)S(1)} %collective-permute-done.10.refs_1_, bf16[96,1152]{1,0:T(8,128)(2,1)S(1)} %collective-permute-done.11.refs_2_, ...), custom_call_target="tpu_custom_call" | custom-call | tf_op jit(solution)/shard_map/pallas_call | solution.py:61
  41.9 0.2 collective-permute-start.13
  42.1 0.0 collective-permute-done.5.refs_2_
  42.1 2.5 %shard_map.258 = (bf16[248,512]{1,0:T(8,128)(2,1)S(1)}, f32[48,128]{1,0:T(8,128)S(1)}) custom-call(s32[6]{0:T(128)S(1)} %pad_add_fusion.ids, bf16[96,1152]{1,0:T(8,128)(2,1)S(1)} %constant_dynamic-update-slice_fusion.refs_0_.column, bf16[96,1152]{1,0:T(8,128)(2,1)S(1)} %collective-permute-done.4.refs_1_, ...), custom_call_target="tpu_custom_call" | custom-call | tf_op jit(solution)/shard_map/pallas_call | solution.py:61
  44.6 0.5 collective-permute-start.7
  45.0 2.1 %shard_map.259 = (bf16[512,1024]{1,0:T(8,128)(2,1)S(1)}, bf16[512,1024]{1,0:T(8,128)(2,1)S(1)}) custom-call(s32[6]{0:T(128)S(1)} %pad_add_fusion.ids, bf16[96,1152]{1,0:T(8,128)(2,1)S(1)} %constant_dynamic-update-slice_fusion.refs_0_.column, bf16[512,2048]{1,0:T(8,128)(2,1)} %down_in.3, bf16[512,2048]{1,0:T(8,128)(2,1)} %bitcast.13), custom_call_target="tpu_custom_call" | custom-call | tf_op jit(solution)/shard_map/pallas_call | solution.py:61
  47.1 0.5 shard_map.263
  47.7 0.5 shard_map.260
  48.2 0.0 collective-permute-done.13.other
  48.2 0.5 shard_map.264
  48.7 0.1 collective-permute-start.14
  48.8 2.0 %collective-permute-start.15 = (bf16[128,1024]{1,0:T(8,128)(2,1)S(1)}, bf16[128,1024]{1,0:T(8,128)(2,1)S(1)}, u32[]{:S(2)}, u32[]{:S(2)}) collective-permute-start(bf16[128,1024]{1,0:T(8,128)(2,1)S(1)} %get-tuple-element.53), channel_id=1, source_target_pairs={{0,4},{2,6},{4,0},{6,2},{8,12},{10,14},{12,8},{14,10},{16,20},{18,... | collective-permute-start | bytes 786440 | tf_op jit(solution)/shard_map/ppermute | solution.py:488
  50.9 0.5 shard_map.261
  51.4 1.5 %collective-permute-start.16 = (bf16[128,1024]{1,0:T(8,128)(2,1)S(1)}, bf16[128,1024]{1,0:T(8,128)(2,1)S(1)}, u32[]{:S(2)}, u32[]{:S(2)}) collective-permute-start(bf16[128,1024]{1,0:T(8,128)(2,1)S(1)} %get-tuple-element.54), channel_id=1, source_target_pairs={{0,6},{2,4},{4,2},{6,0},{8,14},{10,12},{12,10},{14,8},{16,22},{18,... | collective-permute-start | bytes 786440 | tf_op jit(solution)/shard_map/ppermute | solution.py:488
  52.9 0.6 copy.61
  53.5 0.6 copy.62
  54.1 0.7 copy.56
  54.7 0.8 %shard_map.265.refs_4_ = bf16[4,64,24]{2,1,0:T(8,128)(2,1)S(1)} custom-call(s32[6]{0:T(128)S(1)} %pad_add_fusion.ids, bf16[96,1152]{1,0:T(8,128)(2,1)S(1)} %constant_dynamic-update-slice_fusion.refs_0_.column), custom_call_target="tpu_custom_call" | custom-call | tf_op jit(solution)/shard_map/pallas_call | solution.py:61
  55.5 2.5 %collective-permute-done.14.refs_1_ = bf16[128,1024]{1,0:T(8,128)(2,1)S(1)} collective-permute-done((bf16[128,1024]{1,0:T(8,128)(2,1)S(1)}, bf16[128,1024]{1,0:T(8,128)(2,1)S(1)}, u32[]{:S(2)}, u32[]{:S(2)}) %collective-permute-start.14) | collective-permute-done | bytes 262176 | tf_op jit(solution)/shard_map/ppermute | solution.py:488
  58.0 4.1 %collective-permute-done.15.refs_2_ = bf16[128,1024]{1,0:T(8,128)(2,1)S(1)} collective-permute-done((bf16[128,1024]{1,0:T(8,128)(2,1)S(1)}, bf16[128,1024]{1,0:T(8,128)(2,1)S(1)}, u32[]{:S(2)}, u32[]{:S(2)}) %collective-permute-start.15) | collective-permute-done | bytes 262176 | tf_op jit(solution)/shard_map/ppermute | solution.py:488
  62.1 1.6 %collective-permute-done.16.refs_3_ = bf16[128,1024]{1,0:T(8,128)(2,1)S(1)} collective-permute-done((bf16[128,1024]{1,0:T(8,128)(2,1)S(1)}, bf16[128,1024]{1,0:T(8,128)(2,1)S(1)}, u32[]{:S(2)}, u32[]{:S(2)}) %collective-permute-start.16) | collective-permute-done | bytes 262176 | tf_op jit(solution)/shard_map/ppermute | solution.py:488
  63.7 0.3 shard_map.266
  64.0 0.9 %collective-permute-start.17 = (bf16[40,1024]{1,0:T(8,128)(2,1)S(1)}, bf16[40,1024]{1,0:T(8,128)(2,1)S(1)}, u32[]{:S(2)}, u32[]{:S(2)}) collective-permute-start(bf16[40,1024]{1,0:T(8,128)(2,1)S(1)} %get-tuple-element.56), channel_id=1, source_target_pairs={{0,8},{2,10},{4,12},{6,14},{8,0},{10,2},{12,4},{14,6},{16,24},{18,... | collective-permute-start | bytes 245768 | tf_op jit(solution)/shard_map/ppermute | solution.py:488
  64.9 2.2 %collective-permute-start.18 = (bf16[40,1024]{1,0:T(8,128)(2,1)S(1)}, bf16[40,1024]{1,0:T(8,128)(2,1)S(1)}, u32[]{:S(2)}, u32[]{:S(2)}) collective-permute-start(bf16[40,1024]{1,0:T(8,128)(2,1)S(1)} %get-tuple-element.57), channel_id=1, source_target_pairs={{0,16},{2,18},{4,20},{6,22},{8,24},{10,26},{12,28},{14,30},{16,0},... | collective-permute-start | bytes 245768 | tf_op jit(solution)/shard_map/ppermute | solution.py:488
  67.1 1.3 %collective-permute-start.19 = (bf16[40,1024]{1,0:T(8,128)(2,1)S(1)}, bf16[40,1024]{1,0:T(8,128)(2,1)S(1)}, u32[]{:S(2)}, u32[]{:S(2)}) collective-permute-start(bf16[40,1024]{1,0:T(8,128)(2,1)S(1)} %get-tuple-element.58), channel_id=1, source_target_pairs={{0,24},{2,26},{4,28},{6,30},{8,16},{10,18},{12,20},{14,22},{16,8},... | collective-permute-start | bytes 245768 | tf_op jit(solution)/shard_map/ppermute | solution.py:488
  68.5 0.7 collective-permute-done.17.refs_2_
  69.2 4.4 %collective-permute-done.18.refs_3_ = bf16[40,1024]{1,0:T(8,128)(2,1)S(1)} collective-permute-done((bf16[40,1024]{1,0:T(8,128)(2,1)S(1)}, bf16[40,1024]{1,0:T(8,128)(2,1)S(1)}, u32[]{:S(2)}, u32[]{:S(2)}) %collective-permute-start.18) | collective-permute-done | bytes 81952 | tf_op jit(solution)/shard_map/ppermute | solution.py:488
  73.5 0.0 collective-permute-done.19.refs_4_
  73.5 0.8 %shard_map.267 = bf16[24,1024]{1,0:T(8,128)(2,1)S(1)} custom-call(s32[4]{0:T(128)S(1)} %iota_xor_fusion.refs_0_, bf16[40,1024]{1,0:T(8,128)(2,1)S(1)} %get-tuple-element.55.refs_1_, bf16[40,1024]{1,0:T(8,128)(2,1)S(1)} %collective-permute-done.17.refs_2_, bf16[40,1024]{1,0:T(8,128)(2,1)S(1)} %collective-permute-done.18.refs_3_, ...), custom_call_target="tpu_custom_call" | custom-call | tf_op jit(solution)/shard_map/pallas_call | solution.py:61
  74.4 0.6 copy.60
  (21 shorter events, 0.1 us)
Async XLA Ops:
  0.7 7.3 %copy-start.3 = (s32[24,2]{0,1:T(2,128)S(1)}, s32[24,2]{0,1:T(2,128)}, u32[]{:S(2)}) copy-start(s32[24,2]{0,1:T(2,128)} %param.43) | copy-start | bytes 580
  0.7 7.4 %copy-start.4 = (f32[24,2]{0,1:T(2,128)S(1)}, f32[24,2]{0,1:T(2,128)}, u32[]{:S(2)}) copy-start(f32[24,2]{0,1:T(2,128)} %param.44) | copy-start | bytes 580
  0.7 8.2 %copy-start = (bf16[24,2048]{1,0:T(8,128)(2,1)S(1)}, bf16[24,2048]{1,0:T(8,128)(2,1)}, u32[]{:S(2)}) copy-start(bf16[24,2048]{1,0:T(8,128)(2,1)} %tokens.1) | copy-start | bytes 294916
  0.8 8.2 %copy-start.1 = (bf16[2048]{0:T(1024)(128)(2,1)S(1)}, bf16[2048]{0:T(1024)(128)(2,1)}, u32[]{:S(2)}) copy-start(bf16[2048]{0:T(1024)(128)(2,1)} %gain.1) | copy-start | bytes 12292
  0.8 8.2 %copy-start.2 = (bf16[2048]{0:T(1024)(128)(2,1)S(1)}, bf16[2048]{0:T(1024)(128)(2,1)}, u32[]{:S(2)}) copy-start(bf16[2048]{0:T(1024)(128)(2,1)} %branch_gate.1) | copy-start | bytes 12292
  7.5 1.5 %collective-permute-start = (bf16[24,2048]{1,0:T(8,128)(2,1)S(1)}, bf16[24,2048]{1,0:T(8,128)(2,1)S(1)}, u32[]{:S(2)}, u32[]{:S(2)}) collective-permute-start(bf16[24,2048]{1,0:T(8,128)(2,1)S(1)} %get-tuple-element.34.part_a), channel_id=1, source_target_pairs={{0,1},{1,0},{2,3},{3,2},{4,5},{5,4},{6,7},{7,6},{8,9},{9,8},{10,11... | collective-permute-start | bytes 294920 | tf_op jit(solution)/shard_map/ppermute | solution.py:485
  14.5 33.7 %collective-permute-start.8 = (bf16[1024,1024]{1,0:T(8,128)(2,1)S(1)}, bf16[1024,1024]{1,0:T(8,128)(2,1)S(1)}, u32[]{:S(2)}, u32[]{:S(2)}) collective-permute-start(bf16[1024,1024]{1,0:T(8,128)(2,1)S(1)} %get-tuple-element.45), channel_id=1, source_target_pairs={{0,1},{1,0},{2,3},{3,2},{4,5},{5,4},{6,7},{7,6},{8,9},{9,8},{10,11... | collective-permute-start | bytes 6291464 | tf_op jit(solution)/shard_map/ppermute | solution.py:485
  14.9 10.1 %collective-permute-start.3 = (bf16[24,1152]{1,0:T(8,128)(2,1)S(1)}, bf16[24,1152]{1,0:T(8,128)(2,1)S(1)}, u32[]{:S(2)}, u32[]{:S(2)}) collective-permute-start(bf16[24,1152]{1,0:T(8,128)(2,1)S(1)} %get-tuple-element.35.anchor), channel_id=1, source_target_pairs={{0,24},{2,26},{4,28},{6,30},{8,16},{10,18},{12,20},{14,22},{16,8},... | collective-permute-start | bytes 165896 | tf_op jit(solution)/shard_map/ppermute | solution.py:488
  19.7 5.4 %collective-permute-start.2 = (bf16[24,1152]{1,0:T(8,128)(2,1)S(1)}, bf16[24,1152]{1,0:T(8,128)(2,1)S(1)}, u32[]{:S(2)}, u32[]{:S(2)}) collective-permute-start(bf16[24,1152]{1,0:T(8,128)(2,1)S(1)} %get-tuple-element.35.anchor), channel_id=1, source_target_pairs={{0,16},{2,18},{4,20},{6,22},{8,24},{10,26},{12,28},{14,30},{16,0},... | collective-permute-start | bytes 165896 | tf_op jit(solution)/shard_map/ppermute | solution.py:488
  19.7 5.3 %collective-permute-start.1 = (bf16[24,1152]{1,0:T(8,128)(2,1)S(1)}, bf16[24,1152]{1,0:T(8,128)(2,1)S(1)}, u32[]{:S(2)}, u32[]{:S(2)}) collective-permute-start(bf16[24,1152]{1,0:T(8,128)(2,1)S(1)} %get-tuple-element.35.anchor), channel_id=1, source_target_pairs={{0,8},{2,10},{4,12},{6,14},{8,0},{10,2},{12,4},{14,6},{16,24},{18,... | collective-permute-start | bytes 165896 | tf_op jit(solution)/shard_map/ppermute | solution.py:488
  25.1 8.4 %collective-permute-start.10 = (bf16[96,1152]{1,0:T(8,128)(2,1)S(1)}, bf16[96,1152]{1,0:T(8,128)(2,1)S(1)}, u32[]{:S(2)}, u32[]{:S(2)}) collective-permute-start(bf16[96,1152]{1,0:T(8,128)(2,1)S(1)} %constant_dynamic-update-slice_fusion.refs_0_.column), channel_id=1, source_target_pairs={{0,2},{2,0},{4,6},{6,4},{8,10},{10,8},{12,14},{14,12},{16,18},{18,... | collective-permute-start | bytes 663560 | tf_op jit(solution)/shard_map/ppermute | solution.py:488
  26.6 11.3 %collective-permute-start.9 = (bf16[96,1152]{1,0:T(8,128)(2,1)S(1)}, bf16[96,1152]{1,0:T(8,128)(2,1)S(1)}, u32[]{:S(2)}, u32[]{:S(2)}) collective-permute-start(bf16[96,1152]{1,0:T(8,128)(2,1)S(1)} %constant_dynamic-update-slice_fusion.refs_0_.column), channel_id=1, source_target_pairs={{0,4},{2,6},{4,0},{6,2},{8,12},{10,14},{12,8},{14,10},{16,20},{18,... | collective-permute-start | bytes 663560 | tf_op jit(solution)/shard_map/ppermute | solution.py:488
  28.1 10.3 %collective-permute-start.4 = (bf16[96,1152]{1,0:T(8,128)(2,1)S(1)}, bf16[96,1152]{1,0:T(8,128)(2,1)S(1)}, u32[]{:S(2)}, u32[]{:S(2)}) collective-permute-start(bf16[96,1152]{1,0:T(8,128)(2,1)S(1)} %constant_dynamic-update-slice_fusion.refs_0_.column), channel_id=1, source_target_pairs={{0,6},{2,4},{4,2},{6,0},{8,14},{10,12},{12,10},{14,8},{16,22},{18,... | collective-permute-start | bytes 663560 | tf_op jit(solution)/shard_map/ppermute | solution.py:488
  33.4 5.0 %collective-permute-start.12 = (bf16[96,1152]{1,0:T(8,128)(2,1)S(1)}, bf16[96,1152]{1,0:T(8,128)(2,1)S(1)}, u32[]{:S(2)}, u32[]{:S(2)}) collective-permute-start(bf16[96,1152]{1,0:T(8,128)(2,1)S(1)} %collective-permute-done.10.refs_1_), channel_id=1, source_target_pairs={{0,1},{1,0},{2,3},{3,2},{4,5},{5,4},{6,7},{7,6},{8,9},{9,8},{10,11... | collective-permute-start | bytes 663560 | tf_op jit(solution)/shard_map/ppermute | solution.py:485
  38.0 1.5 %collective-permute-start.11 = (bf16[96,1152]{1,0:T(8,128)(2,1)S(1)}, bf16[96,1152]{1,0:T(8,128)(2,1)S(1)}, u32[]{:S(2)}, u32[]{:S(2)}) collective-permute-start(bf16[96,1152]{1,0:T(8,128)(2,1)S(1)} %collective-permute-done.9.refs_0_), channel_id=1, source_target_pairs={{0,1},{1,0},{2,3},{3,2},{4,5},{5,4},{6,7},{7,6},{8,9},{9,8},{10,11... | collective-permute-start | bytes 663560 | tf_op jit(solution)/shard_map/ppermute | solution.py:485
  38.0 4.1 %collective-permute-start.5 = (bf16[96,1152]{1,0:T(8,128)(2,1)S(1)}, bf16[96,1152]{1,0:T(8,128)(2,1)S(1)}, u32[]{:S(2)}, u32[]{:S(2)}) collective-permute-start(bf16[96,1152]{1,0:T(8,128)(2,1)S(1)} %constant_dynamic-update-slice_fusion.refs_0_.column), channel_id=1, source_target_pairs={{0,1},{1,0},{2,3},{3,2},{4,5},{5,4},{6,7},{7,6},{8,9},{9,8},{10,11... | collective-permute-start | bytes 663560 | tf_op jit(solution)/shard_map/ppermute | solution.py:485
  38.5 3.6 %collective-permute-start.6 = (bf16[96,1152]{1,0:T(8,128)(2,1)S(1)}, bf16[96,1152]{1,0:T(8,128)(2,1)S(1)}, u32[]{:S(2)}, u32[]{:S(2)}) collective-permute-start(bf16[96,1152]{1,0:T(8,128)(2,1)S(1)} %collective-permute-done.4.refs_1_), channel_id=1, source_target_pairs={{0,1},{1,0},{2,3},{3,2},{4,5},{5,4},{6,7},{7,6},{8,9},{9,8},{10,11... | collective-permute-start | bytes 663560 | tf_op jit(solution)/shard_map/ppermute | solution.py:485
  41.9 6.3 %collective-permute-start.13 = (bf16[248,512]{1,0:T(8,128)(2,1)S(1)}, bf16[248,512]{1,0:T(8,128)(2,1)S(1)}, u32[]{:S(2)}, u32[]{:S(2)}) collective-permute-start(bf16[248,512]{1,0:T(8,128)(2,1)S(1)} %get-tuple-element.48.own), channel_id=1, source_target_pairs={{0,1},{1,0},{2,3},{3,2},{4,5},{5,4},{6,7},{7,6},{8,9},{9,8},{10,11... | collective-permute-start | bytes 761864 | tf_op jit(solution)/shard_map/ppermute | solution.py:485
  44.6 6.3 %collective-permute-start.7 = (bf16[248,512]{1,0:T(8,128)(2,1)S(1)}, bf16[248,512]{1,0:T(8,128)(2,1)S(1)}, u32[]{:S(2)}, u32[]{:S(2)}) collective-permute-start(bf16[248,512]{1,0:T(8,128)(2,1)S(1)} %get-tuple-element.40.own), channel_id=1, source_target_pairs={{0,1},{1,0},{2,3},{3,2},{4,5},{5,4},{6,7},{7,6},{8,9},{9,8},{10,11... | collective-permute-start | bytes 761864 | tf_op jit(solution)/shard_map/ppermute | solution.py:485
  48.7 9.2 %collective-permute-start.14 = (bf16[128,1024]{1,0:T(8,128)(2,1)S(1)}, bf16[128,1024]{1,0:T(8,128)(2,1)S(1)}, u32[]{:S(2)}, u32[]{:S(2)}) collective-permute-start(bf16[128,1024]{1,0:T(8,128)(2,1)S(1)} %get-tuple-element.52), channel_id=1, source_target_pairs={{0,2},{2,0},{4,6},{6,4},{8,10},{10,8},{12,14},{14,12},{16,18},{18,... | collective-permute-start | bytes 786440 | tf_op jit(solution)/shard_map/ppermute | solution.py:488
  48.8 13.3 %collective-permute-start.15 = (bf16[128,1024]{1,0:T(8,128)(2,1)S(1)}, bf16[128,1024]{1,0:T(8,128)(2,1)S(1)}, u32[]{:S(2)}, u32[]{:S(2)}) collective-permute-start(bf16[128,1024]{1,0:T(8,128)(2,1)S(1)} %get-tuple-element.53), channel_id=1, source_target_pairs={{0,4},{2,6},{4,0},{6,2},{8,12},{10,14},{12,8},{14,10},{16,20},{18,... | collective-permute-start | bytes 786440 | tf_op jit(solution)/shard_map/ppermute | solution.py:488
  51.4 12.3 %collective-permute-start.16 = (bf16[128,1024]{1,0:T(8,128)(2,1)S(1)}, bf16[128,1024]{1,0:T(8,128)(2,1)S(1)}, u32[]{:S(2)}, u32[]{:S(2)}) collective-permute-start(bf16[128,1024]{1,0:T(8,128)(2,1)S(1)} %get-tuple-element.54), channel_id=1, source_target_pairs={{0,6},{2,4},{4,2},{6,0},{8,14},{10,12},{12,10},{14,8},{16,22},{18,... | collective-permute-start | bytes 786440 | tf_op jit(solution)/shard_map/ppermute | solution.py:488
  64.0 5.2 %collective-permute-start.17 = (bf16[40,1024]{1,0:T(8,128)(2,1)S(1)}, bf16[40,1024]{1,0:T(8,128)(2,1)S(1)}, u32[]{:S(2)}, u32[]{:S(2)}) collective-permute-start(bf16[40,1024]{1,0:T(8,128)(2,1)S(1)} %get-tuple-element.56), channel_id=1, source_target_pairs={{0,8},{2,10},{4,12},{6,14},{8,0},{10,2},{12,4},{14,6},{16,24},{18,... | collective-permute-start | bytes 245768 | tf_op jit(solution)/shard_map/ppermute | solution.py:488
  64.9 8.6 %collective-permute-start.18 = (bf16[40,1024]{1,0:T(8,128)(2,1)S(1)}, bf16[40,1024]{1,0:T(8,128)(2,1)S(1)}, u32[]{:S(2)}, u32[]{:S(2)}) collective-permute-start(bf16[40,1024]{1,0:T(8,128)(2,1)S(1)} %get-tuple-element.57), channel_id=1, source_target_pairs={{0,16},{2,18},{4,20},{6,22},{8,24},{10,26},{12,28},{14,30},{16,0},... | collective-permute-start | bytes 245768 | tf_op jit(solution)/shard_map/ppermute | solution.py:488
  67.1 6.4 %collective-permute-start.19 = (bf16[40,1024]{1,0:T(8,128)(2,1)S(1)}, bf16[40,1024]{1,0:T(8,128)(2,1)S(1)}, u32[]{:S(2)}, u32[]{:S(2)}) collective-permute-start(bf16[40,1024]{1,0:T(8,128)(2,1)S(1)} %get-tuple-element.58), channel_id=1, source_target_pairs={{0,24},{2,26},{4,28},{6,30},{8,16},{10,18},{12,20},{14,22},{16,8},... | collective-permute-start | bytes 245768 | tf_op jit(solution)/shard_map/ppermute | solution.py:488
